TPU v7x, 32 devices: a whole 2x2x4 slice. The times are simulated.
32 devices in a mesh: fs: 8 (over z, core), tp: 4 (over y, x).
Axes of the slice: x: 2, y: 2, z: 4, core: 2. Of those that a mesh axis runs over, the one named last changes fastest.
Arguments:
- attn_out: bfloat16 [12288, 2048], P('fs', 'tp'), may hold values from -6 to 6
- out_cot: bfloat16 [12288, 4096], P('fs', 'tp'), may hold values from -6 to 6
- latent: bfloat16 [12288, 1024], P('fs', 'tp'), may hold values from -6 to 6
- value_cot: bfloat16 [12288, 2048], P('fs', 'tp'), may hold values from -6 to 6
- out_weight: float32 [2048, 4096], P('fs', 'tp'), may hold values from -0.125 to 0.125
- value_up_matrix: float32 [1024, 2048], P('fs', 'tp'), may hold values from -0.1875 to 0.1875
- out_basis: bfloat16 [2048, 256], P('fs'), as said below
- value_basis: bfloat16 [1024, 256], P('fs'), as said below
- out_mean: float32 [256, 4096], P(None, 'tp'), may hold values from -2660.43 to 2660.43
- out_square: float32 [256, 4096], P(None, 'tp'), may hold values from 12288 to 2457600, as said below
- value_mean: float32 [256, 2048], P(None, 'tp'), may hold values from -2660.43 to 2660.43
- value_square: float32 [256, 2048], P(None, 'tp'), may hold values from 12288 to 2457600, as said below
Outputs:
- out_step: float32 [2048, 4096], P('fs', 'tp')
- out_new: float32 [2048, 4096], P('fs', 'tp')
- out_copy: bfloat16 [2048, 4096], P(None, 'tp')
- out_mean_new: float32 [256, 4096], P(None, 'tp')
- out_square_new: float32 [256, 4096], P(None, 'tp')
- value_step: float32 [1024, 2048], P('fs', 'tp')
- value_new: float32 [1024, 2048], P('fs', 'tp')
- value_copy: bfloat16 [1024, 2048], P(None, 'tp')
- value_mean_new: float32 [256, 2048], P(None, 'tp')
- value_square_new: float32 [256, 2048], P(None, 'tp')
Inputs may be any that keep to these rules, and one draw needn't show every extreme that they name: `out_basis`: factors of full rank, rows of differing scales. `value_basis`: factors of full rank, rows of differing scales. `out_square`: Positive. `value_square`: Positive.
All inputs are finite; a program needn't handle non-finite values.
Results may differ from a plain program's by a relative error of at most 0.012.
Values may be sent and summed in bfloat16 or wider, within the bound.
A program may use at most 64 MiB of HBM per device.

v0:
```python
import functools

import jax
import jax.numpy as jnp
from jax import lax
from jax.experimental import pallas as pl
from jax.experimental.pallas import tpu as pltpu
from jax.sharding import PartitionSpec as P

LEARN_RATE = 0.01
MEAN_DECAY = 0.8
BETA_SQUARE = 0.9
EPS_RMS = 1e-06
MESH = pl.DeviceIdType.MESH
F32, BF16 = jnp.float32, jnp.bfloat16


def moments(proj, mean_in, square_in):
    mean_new = MEAN_DECAY * mean_in + (1.0 - MEAN_DECAY) * proj
    square_new = BETA_SQUARE * square_in + (1.0 - BETA_SQUARE) * proj * proj
    return (mean_new, square_new, mean_new / jnp.sqrt(square_new))


def rcopy(src, dst, send, recv, fs, tp):
    return pltpu.make_async_remote_copy(
        src_ref=src, dst_ref=dst, send_sem=send, recv_sem=recv,
        device_id=(fs, tp), device_id_type=MESH,
    )


class LineGather:
    def __init__(self, own, buf, up, dn, d2, rz, rd, nz, f, t):
        self.own, self.buf, self.nz, self.t, self.f = own, buf, nz, t, f
        self.up, self.dn, self.d2, self.rz, self.rd = up, dn, d2, rz, rd
        self.z, self.c = lax.div(f, 2), lax.rem(f, 2)
        self.partner = f + 1 - 2 * self.c

    def copy(self, kind, zb, src=None):
        block = self.buf.at[zb * 2 + self.c]
        src = block if src is None else src
        if kind == "up":
            return rcopy(src, block, self.up.at[zb], self.rz.at[zb], self.f + 2, self.t)
        if kind == "dn":
            return rcopy(src, block, self.dn.at[zb], self.rz.at[zb], self.f - 2, self.t)
        return rcopy(src, block, self.d2.at[zb], self.rd.at[zb], self.partner, self.t)

    def spread(self, zb, src, up, dn):
        if up:
            @pl.when(self.z < self.nz - 1)
            def _():
                self.copy("up", zb, src).start()
        if dn:
            @pl.when(self.z > 0)
            def _():
                self.copy("dn", zb, src).start()
        self.copy("d2", zb, src).start()

    def begin(self):
        self.spread(self.z, self.own, True, True)

    def step(self, s):
        @pl.when(self.z >= s)
        def _():
            zb = self.z - s
            rcopy(self.buf.at[zb * 2 + self.c], self.buf.at[zb * 2 + self.c], self.up.at[zb],
                  self.rz.at[zb], self.partner, self.t).wait_recv()
            self.spread(zb, None, True, False)

        @pl.when(self.z + s <= self.nz - 1)
        def _():
            zb = self.z + s
            rcopy(self.buf.at[zb * 2 + self.c], self.buf.at[zb * 2 + self.c], self.dn.at[zb],
                  self.rz.at[zb], self.partner, self.t).wait_recv()
            self.spread(zb, None, False, True)

    def arrive(self):
        for zb in range(self.nz):
            block = self.buf.at[zb * 2 + 1 - self.c]
            rcopy(block, block, self.d2.at[zb], self.rd.at[zb], self.partner, self.t).wait_recv()

    def finish(self):
        for zb in range(self.nz):
            self.copy("d2", zb).wait_send()

            @pl.when((self.z >= zb) & (self.z < self.nz - 1))
            def _():
                self.copy("up", zb).wait_send()

            @pl.when((self.z <= zb) & (self.z > 0))
            def _():
                self.copy("dn", zb).wait_send()


def exchange(nf, nt, *refs):
    hbm_in, (b_o, b_v), rest = refs[:10], refs[10:12], refs[12:]
    wg, bg_out, tot_out, dirs_out = (rest[2 * k:2 * k + 2] for k in range(4))
    totals, rest = rest[8], rest[9:]
    held, rest = rest[:10], rest[10:]
    w16, bg, lift, rsb, lifted, part, psend, pbuf, zsend, zbuf, tot, dirs = (
        rest[2 * k:2 * k + 2] for k in range(12))
    (tsend, tbuf, isem, osem, lsem, bsem, wsem, rs_s, rs_r, ag_s, ag_r, p_s, p_r, z_s, z_r,
     g_s, g_r, gd_s, gd_r, t_s, t_r) = rest[24:]
    lefts, rights, weights, means, squares_in = (held[2 * k:2 * k + 2] for k in range(5))
    pair_of = (0, 1)

    nz = nf // 2
    f, t = lax.axis_index("fs"), lax.axis_index("tp")
    z, c = lax.div(f, 2), lax.rem(f, 2)
    partner = f + 1 - 2 * c
    rank = b_o.shape[1]
    tc, seg, per = lefts[0].shape[0] // nt, rank // nf, nf // nt
    peers_t = [lax.rem(t + s, nt) for s in range(1, nt)]
    peers_z = [lax.rem(z + s, nz) for s in range(1, nz)]

    fetch = [pltpu.make_async_copy(hbm_in[k], held[k], isem.at[k]) for k in range(10)]
    for one in fetch:
        one.start()

    barrier = pltpu.get_barrier_semaphore()
    pl.semaphore_signal(barrier, inc=1, device_id=(partner, t), device_id_type=MESH)
    for pz in peers_z:
        pl.semaphore_signal(barrier, inc=1, device_id=(pz * 2 + c, t), device_id_type=MESH)
    for pt in peers_t:
        pl.semaphore_signal(barrier, inc=1, device_id=(f, pt), device_id_type=MESH)
    pl.semaphore_wait(barrier, 1 + len(peers_z) + len(peers_t))

    gb = [LineGather(own, bg[i], *[bsem.at[i, k] for k in range(5)], nz, f, t)
          for i, own in enumerate((b_o, b_v))]
    gw = [LineGather(w16[i], wg[i], *[wsem.at[i, k] for k in range(5)], nz, f, t) for i in pair_of]
    for g in gb:
        g.begin()
    for i, own in enumerate((b_o, b_v)):
        bg[i][f] = own[...]
        fetch[4 + i].wait()
        w16[i][...] = weights[i][...].astype(BF16)
    for s in range(1, nz):
        for g in gb:
            g.step(s)
    mine = [pltpu.make_async_copy(w16[i], wg[i].at[f], lsem.at[i]) for i in pair_of]
    for i in pair_of:
        gw[i].begin()
        mine[i].start()

    for i in pair_of:
        gb[i].arrive()
        fetch[i].wait()
        rows = bg[i][pl.ds(t * per, per)]
        factor = rows.reshape(rows.shape[0] * rows.shape[1], rank)
        waiting = None
        for pt in peers_t + [t]:
            at = pl.ds(pl.multiple_of(pt * tc, tc), tc)
            lift[i][pt] = jnp.dot(lefts[i][at, :], factor, preferred_element_type=F32).astype(BF16)
            if waiting is not None:
                waiting.start()
            waiting = None
            if pt is not t:
                waiting = rcopy(lift[i].at[pt], rsb[i].at[t], rs_s.at[i, pt], rs_r.at[i, t], f, pt)

    third = (nz - 1 + 2) // 3
    steps = list(range(1, nz))

    def weights_on(some):
        for s in some:
            for g in gw:
                g.step(s)

    def contract(i, pt, first):
        at = pl.ds(pl.multiple_of(pt * tc, tc), tc)
        got = lax.dot_general(lifted[i][pt], rights[i][at, :], (((0,), (0,)), ((), ())),
                              preferred_element_type=F32)
        if first:
            part[i][...] = got
        else:
            part[i][...] += got

    def sum_tokens(i):
        total = lift[i][t].astype(F32)
        for pt in peers_t:
            rcopy(lift[i].at[pt], rsb[i].at[pt], rs_s.at[i, pt], rs_r.at[i, pt], f, pt).wait_recv()
            total = total + rsb[i][pt].astype(F32)
        lifted[i][t] = total.astype(BF16)
        for pt in peers_t:
            rcopy(lifted[i].at[t], lifted[i].at[t], ag_s.at[i, pt], ag_r.at[i, t], f, pt).start()
        fetch[2 + i].wait()
        contract(i, t, True)

    def piece(i, core, zz):
        return part[i][pl.ds(pl.multiple_of((core * nz + zz) * seg, seg), seg), :]

    pairs = [rcopy(psend[i], pbuf[i], p_s.at[i], p_r.at[i], partner, t) for i in pair_of]

    def line_send(i):
        for pt in peers_t:
            rcopy(lifted[i].at[pt], lifted[i].at[pt], ag_s.at[i, pt], ag_r.at[i, pt], f, pt).wait_recv()
            contract(i, pt, False)
        for zz in range(nz):
            psend[i][zz] = piece(i, 1 - c, zz).astype(BF16)
        pairs[i].start()
        pairs[i].wait_recv()
        for pz in peers_z:
            zsend[i][pz] = (piece(i, c, pz) + pbuf[i][pz].astype(F32)).astype(BF16)
        for pz in peers_z:
            rcopy(zsend[i].at[pz], zbuf[i].at[z], z_s.at[i, pz], z_r.at[i, z], pz * 2 + c, t).start()

    me = c * nz + z

    def line_sum(i):
        acc = piece(i, c, z) + pbuf[i][z].astype(F32)
        for pz in peers_z:
            rcopy(zsend[i].at[pz], zbuf[i].at[pz], z_s.at[i, pz], z_r.at[i, pz], pz * 2 + c, t).wait_recv()
            acc = acc + zbuf[i][pz].astype(F32)
        tot[i][me] = acc.astype(BF16)
        own = tot[i].at[me]
        for pz in peers_z:
            rcopy(own, own, g_s.at[i, pz], g_r.at[i, z], pz * 2 + c, t).start()
        rcopy(own, own, gd_s.at[i, z], gd_r.at[i, z], partner, t).start()

    def line_take(i):
        for pz in peers_z:
            got = tot[i].at[c * nz + pz]
            rcopy(got, got, g_s.at[i, pz], g_r.at[i, pz], pz * 2 + c, t).wait_recv()
            rcopy(got, got, gd_s.at[i, pz], gd_r.at[i, pz], partner, t).start()
        for zz in range(nz):
            got = tot[i].at[(1 - c) * nz + zz]
            rcopy(got, got, gd_s.at[i, zz], gd_r.at[i, zz], partner, t).wait_recv()

    outs = [[pltpu.make_async_copy(src[i], dst[i], osem.at[k, i])
             for i in pair_of] for k, (src, dst) in enumerate(((bg, bg_out), (tot, tot_out), (dirs, dirs_out)))]

    def direct(i):
        fetch[6 + i].wait()
        fetch[8 + i].wait()
        part[i][...] = tot[i][...].astype(F32).reshape(part[i].shape)
        dirs[i][...] = moments(part[i][...], means[i][...], squares_in[i][...])[2].astype(BF16)

        def squares(g, sums):
            u = jnp.dot(bg[i][g], dirs[i][...], preferred_element_type=F32)
            return sums + jnp.sum(u * u, axis=0, keepdims=True)

        sums = lax.fori_loop(0, nf, squares, jnp.zeros((1, part[i].shape[1]), F32))
        tile = jnp.zeros((8, 128), F32) + jnp.sum(sums, axis=1, keepdims=True)
        tsend[i] = tile
        tbuf[t, i] = tile

    for i in pair_of:
        outs[0][i].start()
    weights_on(steps[:third])
    for i in pair_of:
        sum_tokens(i)
    weights_on(steps[third:2 * third])
    for i in pair_of:
        line_send(i)
    for i in pair_of:
        line_sum(i)
    weights_on(steps[2 * third:])
    for i in pair_of:
        line_take(i)
        direct(i)
    for pt in peers_t:
        rcopy(tsend, tbuf.at[t], t_s.at[pt], t_r.at[t], f, pt).start()
    for k in (1, 2):
        for i in pair_of:
            outs[k][i].start()
    for i in pair_of:
        mine[i].wait()
        gw[i].arrive()
        gb[i].finish()
        gw[i].finish()
        pairs[i].wait_send()
        for pt in peers_t:
            rcopy(lift[i].at[pt], rsb[i].at[t], rs_s.at[i, pt], rs_r.at[i, t], f, pt).wait_send()
            rcopy(lifted[i].at[t], lifted[i].at[t], ag_s.at[i, pt], ag_r.at[i, t], f, pt).wait_send()
        for pz in peers_z:
            rcopy(zsend[i].at[pz], zbuf[i].at[z], z_s.at[i, pz], z_r.at[i, z], pz * 2 + c, t).wait_send()
            own = tot[i].at[me]
            rcopy(own, own, g_s.at[i, pz], g_r.at[i, z], pz * 2 + c, t).wait_send()
        for zz in range(nz):
            got = tot[i].at[c * nz + zz]
            rcopy(got, got, gd_s.at[i, zz], gd_r.at[i, zz], partner, t).wait_send()
        for k in range(3):
            outs[k][i].wait()
    for pt in peers_t:
        rcopy(tsend, tbuf.at[pt], t_s.at[pt], t_r.at[pt], f, pt).wait_recv()
    summed = tbuf[0]
    for k in range(1, nt):
        summed = summed + tbuf[k]
    totals[...] = summed
    for pt in peers_t:
        rcopy(tsend, tbuf.at[t], t_s.at[pt], t_r.at[t], f, pt).wait_send()


def gather_and_reduce(nf, nt, lefts, rights, weights, bases, means, squares):
    rank, nz, tokens = bases[0].shape[1], nf // 2, rights[0].shape[0]
    tc, seg = tokens // nt, rank // nf
    heights, widths = [b.shape[0] for b in bases], [r.shape[1] for r in rights]
    vmem, dma = pl.BlockSpec(memory_space=pltpu.VMEM), pltpu.SemaphoreType.DMA
    hbm = pl.BlockSpec(memory_space=pltpu.HBM)
    fetched = (*lefts, *rights, *weights, *means, *squares)

    def two(shape_of, kind=BF16, make=pltpu.VMEM):
        return [make(shape_of(h, w), kind) for h, w in zip(heights, widths)]

    def outs(shape_of):
        return two(shape_of, make=jax.ShapeDtypeStruct)

    token_chunks = lambda h, w: (nt, tc, rank)
    line_pieces = lambda h, w: (nz, seg, w)
    return pl.pallas_call(
        functools.partial(exchange, nf, nt),
        out_shape=(
            *outs(lambda h, w: (nf, h, w)), *outs(lambda h, w: (nf, h, rank)),
            *outs(lambda h, w: (nf, seg, w)), *outs(lambda h, w: (rank, w)),
            jax.ShapeDtypeStruct((2, 8, 128), F32),
        ),
        in_specs=[hbm] * 10 + [vmem] * 2,
        out_specs=(hbm,) * 8 + (vmem,),
        scratch_shapes=[
            *[pltpu.VMEM(x.shape, x.dtype) for x in fetched],
            *two(lambda h, w: (h, w)), *two(lambda h, w: (nf, h, rank)),
            *two(token_chunks), *two(token_chunks), *two(token_chunks),
            *two(lambda h, w: (rank, w), F32),
            *two(line_pieces), *two(line_pieces), *two(line_pieces), *two(line_pieces),
            *two(lambda h, w: (nf, seg, w)), *two(lambda h, w: (rank, w)),
            pltpu.VMEM((2, 8, 128), F32),
            pltpu.VMEM((nt, 2, 8, 128), F32),
            dma((10,)), dma((3, 2)), dma((2,)), dma((2, 5, nz)), dma((2, 5, nz)),
            dma((2, nt)), dma((2, nt)), dma((2, nt)), dma((2, nt)), dma((2,)), dma((2,)),
            dma((2, nz)), dma((2, nz)), dma((2, nz)), dma((2, nz)), dma((2, nz)), dma((2, nz)),
            dma((nt,)), dma((nt,)),
        ],
        compiler_params=pltpu.CompilerParams(
            collective_id=0, has_side_effects=True, vmem_limit_bytes=56 * 1024 * 1024
        ),
        name="exchange",
    )(*fetched, *bases)


def apply(nt, *refs):
    parts, totals = [refs[8 * i:8 * i + 8] for i in range(2)], refs[16]
    outs = [refs[17 + 5 * i:22 + 5 * i] for i in range(2)]
    g, steps = pl.program_id(0), pl.num_programs(0)
    for i in range(2):
        proj, mean_in, square_in, direction, gathered, factor, basis, weight = parts[i]
        step, new, copy, mean, square = outs[i]
        count = gathered.shape[1] * steps * gathered.shape[2] * nt
        scale = LEARN_RATE * lax.rsqrt(totals[i, 0:1, 0:1] / lax.convert_element_type(count, F32) + EPS_RMS)
        p = proj[0].astype(F32)
        mean[...] = MEAN_DECAY * mean_in[...] + (1.0 - MEAN_DECAY) * p
        square[...] = BETA_SQUARE * square_in[...] + (1.0 - BETA_SQUARE) * p * p
        update = jnp.dot(factor[0], direction[...], preferred_element_type=F32)
        copy[...] = (gathered[0].astype(F32) - scale * update).astype(BF16)

        @pl.when(g == 0)
        def _():
            own = scale * jnp.dot(basis[...], direction[...], preferred_element_type=F32)
            step[...] = own
            new[...] = weight[...] - own


def finish(nf, nt, args, totals):
    whole = lambda x: pl.BlockSpec(x.shape, lambda g: (0,) * x.ndim)
    third = lambda x: pl.BlockSpec((1,) + x.shape[1:], lambda g: (g, 0, 0))
    rows = lambda x: pl.BlockSpec((x.shape[0] // nf, x.shape[1]), lambda g: (g, 0))
    in_specs, out_specs, out_shape = [], [], []
    for proj, mean_in, square_in, direction, gathered, factor, basis, weight in args:
        in_specs += [third(proj), rows(mean_in), rows(square_in), whole(direction), third(gathered),
                     third(factor), whole(basis), whole(weight)]
        copy = jax.ShapeDtypeStruct((nf * weight.shape[0], weight.shape[1]), BF16)
        like = lambda x: jax.ShapeDtypeStruct(x.shape, F32)
        out_shape += [like(weight), like(weight), copy, like(mean_in), like(square_in)]
        out_specs += [whole(weight), whole(weight), rows(copy), rows(mean_in), rows(square_in)]
    return pl.pallas_call(
        functools.partial(apply, nt),
        grid=(nf,),
        in_specs=in_specs + [whole(totals)],
        out_specs=out_specs,
        out_shape=out_shape,
        compiler_params=pltpu.CompilerParams(dimension_semantics=("arbitrary",)),
        name="apply",
    )(*args[0], *args[1], totals)


def per_device(nf, nt, attn_out, out_cot, latent, value_cot, out_weight, value_up_matrix,
               out_basis, value_basis, out_mean, out_square, value_mean, value_square):
    wg_o, wg_v, bg_o, bg_v, tot_o, tot_v, dirs_o, dirs_v, totals = gather_and_reduce(
        nf, nt, (attn_out, latent), (out_cot, value_cot), (out_weight, value_up_matrix),
        (out_basis, value_basis), (out_mean, value_mean), (out_square, value_square))
    return tuple(finish(nf, nt, (
        (tot_o, out_mean, out_square, dirs_o, wg_o, bg_o, out_basis, out_weight),
        (tot_v, value_mean, value_square, dirs_v, wg_v, bg_v, value_basis, value_up_matrix),
    ), totals))


def solution(mesh):
    both, rows, cols = P("fs", "tp"), P("fs", None), P(None, "tp")
    return jax.shard_map(
        functools.partial(per_device, mesh.shape["fs"], mesh.shape["tp"]),
        mesh=mesh,
        in_specs=(both,) * 6 + (rows,) * 2 + (cols,) * 4,
        out_specs=(both, both, cols, cols, cols) * 2,
        check_vma=False,
    )
```

profile of v0, /device:TPU:0, one launch (start us, length us, event | category | flops | bytes accessed | tf_op | source)
XLA Modules:
  0.0 103.1 jit_solution(10514559008447595337)
XLA Ops:
  0.6 88.9 %exchange.1 = (bf16[8,256,1024]{2,1,0:T(8,128)(2,1)}, bf16[8,128,512]{2,1,0:T(8,128)(2,1)}, bf16[8,256,256]{2,1,0:T(8,128)(2,1)}, bf16[8,128,256]{2,1,0:T(8,128)...) custom-call(bf16[1536,512]{1,0:T(8,128)(2,1)} %refs_0_.1, ...), custom_call_target="tpu_custom_call" | custom-call | tf_op jit(solution)/shard_map/exchange/pallas_call | solution.py:308
  89.6 13.5 %apply.1 = (f32[256,1024]{1,0:T(8,128)}, f32[256,1024]{1,0:T(8,128)}, bf16[2048,1024]{1,0:T(8,128)(2,1)}, f32[256,1024]{1,0:T(8,128)}, f32[256,1024]{1,0:T(8,128...) custom-call(bf16[8,32,1024]{2,1,0:T(8,128)(2,1)} %get-tuple-element., ...), custom_call_target="tpu_custom_call" | custom-call | tf_op jit(solution)/shard_map/apply/pallas_call | solution.py:372
where the time goes:
time: 103 us
  Pallas kernels  102 us (99%)
    pallas_call x1, Pallas kernels, gather_and_reduce(): pl.pallas_call(functools.partial(exchange, nf, nt), out_shape=(*outs(lamb...  88.9 us
    pallas_call x1, Pallas kernels, finish(): pl.pallas_call(functools.partial(apply, nt), grid=(nf,), in_specs=in_spec...  13.5 us

commit v1 on v0

v1 whole, which is shorter than its diff:
```python
import functools

import jax
import jax.numpy as jnp
from jax import lax
from jax.experimental import pallas as pl
from jax.experimental.pallas import tpu as pltpu
from jax.sharding import PartitionSpec as P

LEARN_RATE = 0.01
MEAN_DECAY = 0.8
BETA_SQUARE = 0.9
EPS_RMS = 1e-06
MESH = pl.DeviceIdType.MESH
F32, BF16 = jnp.float32, jnp.bfloat16
PAIR = (0, 1)
CORES = 2
NEAR = (((1, 0),), ((1, 1), (1, 2)), ((2, 0),), ((2, 1),), ((2, 2),))


def rcopy(src, dst, send, recv, fs, tp):
    return pltpu.make_async_remote_copy(
        src_ref=src, dst_ref=dst, send_sem=send, recv_sem=recv,
        device_id=(fs, tp), device_id_type=MESH,
    )


def over_rows(left, right):
    return lax.dot_general(left, right, (((0,), (0,)), ((), ())), preferred_element_type=F32)


def exchange(nf, nt, *refs):
    hbm, rest = refs[:12], refs[12:]
    wg, bg, dirs, mean_new, square_new, w32 = (rest[2 * k:2 * k + 2] for k in range(6))
    totals, rest = rest[12], rest[13:]
    left, right, mean, square, sbuf, rbuf, kept, lifted, part, psend, pbuf, zsend, zbuf, tot, gram = (
        rest[2 * k:2 * k + 2] for k in range(15))
    (tsend, tbuf, isem, b_s, b_r, bd_s, bd_r, c_s, c_r, w_u, w_d, w_r, wd_s, wd_r,
     rs_s, rs_r, ag_s, ag_r, p_s, p_r, z_s, z_r, g_s, g_r, gd_s, gd_r, t_s, t_r) = rest[30:]

    nz = nf // CORES
    f, t = lax.axis_index("fs"), lax.axis_index("tp")
    z, c = lax.div(f, CORES), lax.rem(f, CORES)
    partner = f + 1 - 2 * c
    rank = bg[0].shape[2]
    tokens, seg = left[0].shape[0], rank // nf
    peers_t = [lax.rem(t + s, nt) for s in range(1, nt)]
    peers_z = [lax.rem(z + s, nz) for s in range(1, nz)]
    own_column = z == t

    held = (*left, *right, *w32, *[b.at[f] for b in bg], *mean, *square)
    order = (6, 7, 4, 5, 0, 1, 2, 3, 8, 9, 10, 11)
    fetch = [pltpu.make_async_copy(hbm[k], held[k], isem.at[k]) for k in range(12)]
    for k in order:
        fetch[k].start()

    barrier = pltpu.get_barrier_semaphore()
    pl.semaphore_signal(barrier, inc=1, device_id=(partner, t), device_id_type=MESH)
    for pz in peers_z:
        pl.semaphore_signal(barrier, inc=1, device_id=(pz * CORES + c, t), device_id_type=MESH)
    for pt in peers_t:
        pl.semaphore_signal(barrier, inc=1, device_id=(f, pt), device_id_type=MESH)
    pl.semaphore_wait(barrier, 1 + len(peers_z) + len(peers_t))

    lane = t * CORES + c
    other = t * CORES + 1 - c

    def basis_line(i, zz):
        block = bg[i].at[lane]
        return rcopy(block, block, b_s.at[i, zz], b_r.at[i], zz * CORES + c, t)

    def basis_core(i, block):
        ref = bg[i].at[block]
        return rcopy(ref, ref, bd_s.at[i, block], bd_r.at[i, block], partner, t)

    def basis_plane(i, pt, block):
        ref = bg[i].at[block]
        return rcopy(ref, ref, c_s.at[i, pt], c_r.at[i, lax.div(block, CORES)], f, pt)

    for i in PAIR:
        fetch[6 + i].wait()

        @pl.when(own_column)
        def _():
            for dist in range(nz - 1, 0, -1):
                for zz, there in ((z + dist, z + dist < nz), (z - dist, z - dist >= 0)):
                    @pl.when(there)
                    def _():
                        basis_line(i, zz).start()
        basis_core(i, f).start()
    for i in PAIR:
        fetch[4 + i].wait()
        wg[i][f] = w32[i][...].astype(BF16)

    heights = [w.shape[1] for w in wg]
    tall = min(heights)
    units = [(i, r) for i in PAIR for r in range(0, heights[i], tall)]

    def unit(u, zb, core):
        i, r = units[u]
        return wg[i].at[zb * CORES + core, pl.ds(r, tall)]

    def w_up(u, zb):
        ref = unit(u, zb, c)
        return rcopy(ref, ref, w_u.at[u, zb], w_r.at[u, zb], f + CORES, t)

    def w_dn(u, zb):
        ref = unit(u, zb, c)
        return rcopy(ref, ref, w_d.at[u, zb], w_r.at[u, zb], f - CORES, t)

    def w_core(u, zb, core):
        ref = unit(u, zb, core)
        return rcopy(ref, ref, wd_s.at[u, zb], wd_r.at[u, zb], partner, t)

    def pass_on(u, zb, up, down):
        if up:
            @pl.when(z < nz - 1)
            def _():
                w_up(u, zb).start()
        if down:
            @pl.when(z > 0)
            def _():
                w_dn(u, zb).start()

    def weights_on(events):
        for s, u in events:
            if s > nz - 1:
                continue

            @pl.when(z >= s)
            def _():
                w_up(u, z - s).wait_recv()
                pass_on(u, z - s, True, False)
                w_core(u, z - s, c).start()

            @pl.when(z + s <= nz - 1)
            def _():
                w_dn(u, z + s).wait_recv()
                pass_on(u, z + s, False, True)
                w_core(u, z + s, c).start()

    for i in PAIR:
        @pl.when(jnp.logical_not(own_column))
        def _():
            basis_line(i, z).wait_recv()
            basis_core(i, lane).start()
        if i == 0:
            for u in range(len(units)):
                pass_on(u, z, True, True)

    levels = nt.bit_length() - 1
    sizes = [tokens // 2 >> k for k in range(levels + 1)]
    offs = [sizes[0] - s for s in sizes]
    masks = [[1 << k for k in range(levels)], [1 << k for k in reversed(range(levels))]]
    bits = [[lax.rem(lax.div(t, m), 2) for m in masks[h]] for h in PAIR]
    mates = [[t + m * (1 - 2 * b) for m, b in zip(masks[h], bits[h])] for h in PAIR]
    bases = []
    for h in PAIR:
        at = [h * sizes[0]]
        for k in range(levels):
            at.append(at[-1] + bits[h][k] * sizes[k + 1])
        bases.append(at)

    def rows(start, size):
        return pl.ds(pl.multiple_of(start, 16), size)

    def away(h, k):
        return rows(bases[h][k] + (1 - bits[h][k]) * sizes[k + 1], sizes[k + 1])

    def rs(i, h, k):
        at = pl.ds(offs[k], sizes[k + 1])
        return rcopy(sbuf[i].at[h, at], rbuf[i].at[h, at], rs_s.at[i, h, k], rs_r.at[i, h, k], f, mates[h][k])

    def ag(i, h, k, received=False):
        ref = lifted[i].at[away(h, k) if received else rows(bases[h][k + 1], sizes[k + 1])]
        return rcopy(ref, ref, ag_s.at[i, h, k], ag_r.at[i, h, k], f, mates[h][k])

    def lift_tokens(i):
        two = bg[i][pl.ds(t * CORES, CORES)]
        factor = two.reshape(two.shape[0] * two.shape[1], rank)
        for h in PAIR:
            sbuf[i][h, pl.ds(0, sizes[1])] = jnp.dot(
                left[i][away(h, 0), :], factor, preferred_element_type=F32).astype(BF16)
            rs(i, h, 0).start()
        for h in PAIR:
            kept[i][h, pl.ds(0, sizes[1])] = jnp.dot(
                left[i][rows(bases[h][1], sizes[1]), :], factor, preferred_element_type=F32)

    def contract(i, at, first=False):
        got = over_rows(lifted[i][at, :], right[i][at, :])
        if first:
            part[i][...] = got
        else:
            part[i][...] += got

    def halve(i, k):
        for h in PAIR:
            rs(i, h, k).wait_recv()
            if k + 1 < levels:
                small = sizes[k + 2]
                for b, mine in ((1 - bits[h][k + 1], False), (bits[h][k + 1], True)):
                    at = rows(offs[k] + b * small, small)
                    both = kept[i][h, at] + rbuf[i][h, at].astype(F32)
                    to = pl.ds(offs[k + 1], small)
                    if mine:
                        kept[i][h, to] = both
                    else:
                        sbuf[i][h, to] = both.astype(BF16)
                        rs(i, h, k + 1).start()
            else:
                at = pl.ds(offs[k], sizes[k + 1])
                lifted[i][rows(bases[h][k + 1], sizes[k + 1]), :] = (
                    kept[i][h, at] + rbuf[i][h, at].astype(F32)).astype(BF16)
                ag(i, h, k).start()
        if k + 1 == levels:
            fetch[2 + i].wait()
            for h in PAIR:
                contract(i, rows(bases[h][levels], sizes[levels]), h == 0)

    def double(i, k):
        for h in PAIR:
            ag(i, h, k, True).wait_recv()
            if k > 0:
                ag(i, h, k - 1).start()
        for h in PAIR:
            contract(i, away(h, k))

    def piece(i, core, zz):
        return part[i][pl.ds(pl.multiple_of((core * nz + zz) * seg, seg), seg), :]

    pairs = [rcopy(psend[i], pbuf[i], p_s.at[i], p_r.at[i], partner, t) for i in PAIR]
    me = c * nz + z

    def pair_send(i):
        for zz in range(nz):
            psend[i][zz] = piece(i, 1 - c, zz).astype(BF16)
        pairs[i].start()

    def line(i, pz):
        return rcopy(zsend[i].at[pz], zbuf[i].at[z], z_s.at[i, pz], z_r.at[i, z], pz * CORES + c, t)

    def line_got(i, pz):
        return rcopy(zsend[i].at[pz], zbuf[i].at[pz], z_s.at[i, pz], z_r.at[i, pz], pz * CORES + c, t)

    def share(i, pz, at):
        ref = tot[i].at[at]
        return rcopy(ref, ref, g_s.at[i, pz], g_r.at[i, at - c * nz], pz * CORES + c, t)

    def share_core(i, core, zz):
        ref = tot[i].at[core * nz + zz]
        return rcopy(ref, ref, gd_s.at[i, zz], gd_r.at[i, zz], partner, t)

    def line_send(i):
        pairs[i].wait_recv()
        for pz in peers_z:
            zsend[i][pz] = (piece(i, c, pz) + pbuf[i][pz].astype(F32)).astype(BF16)
            line(i, pz).start()

    def line_sum(i):
        acc = piece(i, c, z) + pbuf[i][z].astype(F32)
        for pz in peers_z:
            line_got(i, pz).wait_recv()
            acc = acc + zbuf[i][pz].astype(F32)
        tot[i][me] = acc.astype(BF16)
        for pz in peers_z:
            share(i, pz, me).start()
        share_core(i, c, z).start()

    def line_take(i):
        for pz in peers_z:
            share(i, pz, c * nz + pz).wait_recv()
            share_core(i, c, pz).start()

    def squared(i):
        flat = bg[i][...].reshape(nf * bg[i].shape[1], rank)
        full = over_rows(flat, flat)
        high = full.astype(BF16)
        gram[i][0] = high
        gram[i][1] = (full - high.astype(F32)).astype(BF16)

    def direct(i):
        for zz in range(nz):
            share_core(i, 1 - c, zz).wait_recv()
        proj = tot[i][...].astype(F32).reshape(part[i].shape)
        mean_out = MEAN_DECAY * mean[i][...] + (1.0 - MEAN_DECAY) * proj
        square_out = BETA_SQUARE * square[i][...] + (1.0 - BETA_SQUARE) * proj * proj
        mean_new[i][...] = mean_out
        square_new[i][...] = square_out
        d = (mean_out / jnp.sqrt(square_out)).astype(BF16)
        dirs[i][...] = d
        turned = (jnp.dot(gram[i][0], d, preferred_element_type=F32)
                  + jnp.dot(gram[i][1], d, preferred_element_type=F32))
        sums = jnp.sum(d.astype(F32) * turned, axis=0, keepdims=True)
        tile = jnp.zeros((8, 128), F32) + jnp.sum(sums, axis=1, keepdims=True)
        tsend[i] = tile
        tbuf[t, i] = tile

    def plane_send(i):
        @pl.when(jnp.logical_not(own_column))
        def _():
            for pt in peers_t:
                basis_plane(i, pt, lane).start()

    def plane_take(i):
        for pt in peers_t:
            @pl.when(pt != z)
            def _():
                basis_plane(i, pt, pt * CORES + c).wait_recv()
                basis_core(i, pt * CORES + c).start()
        for pt in peers_t:
            basis_core(i, pt * CORES + 1 - c).wait_recv()

    for i in PAIR:
        fetch[i].wait()
        basis_core(i, other).wait_recv()
        lift_tokens(i)
    for u in range(len(units)):
        w_core(u, z, c).start()

    points = list(NEAR)
    for k in range(levels):
        for i in PAIR:
            halve(i, k)
            if k < 1:
                weights_on(points.pop(0))
    weights_on(points.pop(0))
    for k in range(levels - 1, 0, -1):
        for i in PAIR:
            double(i, k)
    double(0, 0)
    pair_send(0)
    line_send(0)
    weights_on(points.pop(0))
    double(1, 0)
    pair_send(1)
    line_send(1)
    for i in PAIR:
        plane_send(i)
    line_sum(0)
    line_sum(1)
    weights_on(points.pop(0))
    for i in PAIR:
        plane_take(i)
        squared(i)
    for i in PAIR:
        fetch[8 + i].wait()
        fetch[10 + i].wait()
    for i in PAIR:
        line_take(i)
    for i in PAIR:
        direct(i)
    for pt in peers_t:
        rcopy(tsend, tbuf.at[t], t_s.at[pt], t_r.at[t], f, pt).start()
    weights_on([(s, u) for s in range(3, nz) for u in range(len(units))])

    for pt in peers_t:
        rcopy(tsend, tbuf.at[pt], t_s.at[pt], t_r.at[pt], f, pt).wait_recv()
    summed = tbuf[0]
    for k in range(1, nt):
        summed = summed + tbuf[k]
    totals[...] = summed

    for u in range(len(units)):
        for zb in range(nz):
            w_core(u, zb, 1 - c).wait_recv()
    for i in PAIR:
        @pl.when(own_column)
        def _():
            for pz in peers_z:
                basis_line(i, pz).wait_send()

        @pl.when(jnp.logical_not(own_column))
        def _():
            basis_core(i, lane).wait_send()
            for pt in peers_t:
                basis_plane(i, pt, lane).wait_send()
        basis_core(i, f).wait_send()
        for pt in peers_t:
            @pl.when(pt != z)
            def _():
                basis_core(i, pt * CORES + c).wait_send()
        for h in PAIR:
            for k in range(levels):
                rs(i, h, k).wait_send()
                ag(i, h, k).wait_send()
        pairs[i].wait_send()
        for pz in peers_z:
            line(i, pz).wait_send()
            share(i, pz, me).wait_send()
        for zz in range(nz):
            share_core(i, c, zz).wait_send()
    for u in range(len(units)):
        for zb in range(nz):
            w_core(u, zb, c).wait_send()

            @pl.when((z >= zb) & (z < nz - 1))
            def _():
                w_up(u, zb).wait_send()

            @pl.when((z <= zb) & (z > 0))
            def _():
                w_dn(u, zb).wait_send()
    for pt in peers_t:
        rcopy(tsend, tbuf.at[t], t_s.at[pt], t_r.at[t], f, pt).wait_send()


def gather_and_reduce(nf, nt, lefts, rights, weights, bases, means, squares):
    rank, nz, tokens = bases[0].shape[1], nf // CORES, rights[0].shape[0]
    seg, levels = rank // nf, nt.bit_length() - 1
    heights, widths = [b.shape[0] for b in bases], [r.shape[1] for r in rights]
    units = sum(heights) // min(heights)
    vmem, dma = pl.BlockSpec(memory_space=pltpu.VMEM), pltpu.SemaphoreType.DMA
    hbm = pl.BlockSpec(memory_space=pltpu.HBM)

    def two(shape_of, kind=BF16, make=pltpu.VMEM):
        return [make(shape_of(h, w), kind) for h, w in zip(heights, widths)]

    def outs(shape_of, kind=BF16):
        return two(shape_of, kind, jax.ShapeDtypeStruct)

    halves = lambda h, w: (2, tokens // 2, rank)
    line_pieces = lambda h, w: (nz, seg, w)
    ranked = lambda h, w: (rank, w)
    fetched = (*lefts, *rights, *means, *squares)
    return pl.pallas_call(
        functools.partial(exchange, nf, nt),
        out_shape=(
            *outs(lambda h, w: (nf, h, w)), *outs(lambda h, w: (nf, h, rank)), *outs(ranked),
            *outs(ranked, F32), *outs(ranked, F32), *outs(lambda h, w: (h, w), F32),
            jax.ShapeDtypeStruct((2, 8, 128), F32),
        ),
        in_specs=[hbm] * 12,
        out_specs=(vmem,) * 13,
        scratch_shapes=[
            *[pltpu.VMEM(x.shape, x.dtype) for x in fetched],
            *two(halves), *two(halves), *two(halves, F32), *two(lambda h, w: (tokens, rank)), *two(ranked, F32),
            *two(line_pieces), *two(line_pieces), *two(line_pieces), *two(line_pieces),
            *two(lambda h, w: (nf, seg, w)), *two(lambda h, w: (2, rank, rank)),
            pltpu.VMEM((2, 8, 128), F32),
            pltpu.VMEM((nt, 2, 8, 128), F32),
            dma((12,)), dma((2, nz)), dma((2,)), dma((2, nf)), dma((2, nf)), dma((2, nt)), dma((2, nt)),
            *[dma((units, nz))] * 5,
            *[dma((2, 2, levels))] * 4,
            dma((2,)), dma((2,)), *[dma((2, nz))] * 6, dma((nt,)), dma((nt,)),
        ],
        compiler_params=pltpu.CompilerParams(
            collective_id=0, has_side_effects=True, vmem_limit_bytes=40 * 1024 * 1024
        ),
        name="exchange",
    )(*[pltpu.with_memory_space_constraint(x, pltpu.HBM)
        for x in (*lefts, *rights, *weights, *bases, *means, *squares)])


def apply(nf, nt, *refs):
    wg, bg, dirs, mean_new, square_new, w32 = (refs[2 * k:2 * k + 2] for k in range(6))
    totals = refs[12]
    outs = [refs[13 + 5 * i:18 + 5 * i] for i in PAIR]
    step, new, copy = (refs[23 + 2 * k:25 + 2 * k] for k in range(3))
    sem, csem = refs[29:]
    f = lax.axis_index("fs")

    def to(k, i):
        src = (step, new, None, mean_new, square_new)[k]
        return pltpu.make_async_copy(src[i], outs[i][k], sem.at[i, k])

    def block(i, g):
        height = w32[i].shape[0]
        return pltpu.make_async_copy(copy[i].at[pl.ds(g * height, height)],
                                     outs[i][2].at[pl.ds(g * height, height)], csem.at[i, g])

    for i in PAIR:
        to(3, i).start()
        to(4, i).start()
    scales = []
    for i in PAIR:
        count = w32[i].shape[0] * nf * w32[i].shape[1] * nt
        scale = LEARN_RATE * lax.rsqrt(totals[i, 0:1, 0:1] / lax.convert_element_type(count, F32) + EPS_RMS)
        scales.append(scale)
        own = scale * jnp.dot(bg[i][f], dirs[i][...], preferred_element_type=F32)
        step[i][...] = own
        new[i][...] = w32[i][...] - own
        to(0, i).start()
        to(1, i).start()
    for i in PAIR:
        height = w32[i].shape[0]
        for g in range(nf):
            update = jnp.dot(bg[i][g], dirs[i][...], preferred_element_type=F32)
            copy[i][pl.ds(g * height, height), :] = (wg[i][g].astype(F32) - scales[i] * update).astype(BF16)
            block(i, g).start()
    for i in PAIR:
        for k in (0, 1, 3, 4):
            to(k, i).wait()
        for g in range(nf):
            block(i, g).wait()


def finish(nf, nt, gathered):
    w32 = gathered[10:12]
    vmem, hbm = pl.BlockSpec(memory_space=pltpu.VMEM), pl.BlockSpec(memory_space=pltpu.HBM)
    out_shape = []
    for i in PAIR:
        copy = jax.ShapeDtypeStruct((nf * w32[i].shape[0], w32[i].shape[1]), BF16)
        like = lambda x: jax.ShapeDtypeStruct(x.shape, F32)
        out_shape += [like(w32[i]), like(w32[i]), copy, like(gathered[6 + i]), like(gathered[8 + i])]
    return pl.pallas_call(
        functools.partial(apply, nf, nt),
        in_specs=[vmem] * 13,
        out_specs=[hbm] * 10,
        out_shape=out_shape,
        scratch_shapes=[
            *[pltpu.VMEM(w.shape, F32) for w in w32], *[pltpu.VMEM(w.shape, F32) for w in w32],
            *[pltpu.VMEM(out_shape[2 + 5 * i].shape, BF16) for i in PAIR],
            pltpu.SemaphoreType.DMA((2, 5)), pltpu.SemaphoreType.DMA((2, nf)),
        ],
        compiler_params=pltpu.CompilerParams(vmem_limit_bytes=12 * 1024 * 1024),
        name="apply",
    )(*gathered)


def per_device(nf, nt, attn_out, out_cot, latent, value_cot, out_weight, value_up_matrix,
               out_basis, value_basis, out_mean, out_square, value_mean, value_square):
    gathered = gather_and_reduce(
        nf, nt, (attn_out, latent), (out_cot, value_cot), (out_weight, value_up_matrix),
        (out_basis, value_basis), (out_mean, value_mean), (out_square, value_square))
    return tuple(finish(nf, nt, gathered))


def solution(mesh):
    both, rows, cols = P("fs", "tp"), P("fs", None), P(None, "tp")
    return jax.shard_map(
        functools.partial(per_device, mesh.shape["fs"], mesh.shape["tp"]),
        mesh=mesh,
        in_specs=(both,) * 6 + (rows,) * 2 + (cols,) * 4,
        out_specs=(both, both, cols, cols, cols) * 2,
        check_vma=False,
    )
```

time: 103 us -> 84.6 us (0.82)
  Pallas kernels: 102 us -> 83.8 us
    pallas_call x1, Pallas kernels: 88.9 us -> 79 us  [gather_and_reduce(): pl.pallas_call(functools.partial(exchange, nf, nt), out_shape=(*outs(lamb...]
    pallas_call x1, Pallas kernels: 13.5 us -> 4.78 us  [finish(): pl.pallas_call(functools.partial(apply, nf, nt), in_specs=[vmem] * 13, ou...]
where the time goes in v1:
time: 84.6 us; the launch traced here: 84.4 us
  Pallas kernels  83.8 us (99%)
    pallas_call x1, Pallas kernels, gather_and_reduce(): pl.pallas_call(functools.partial(exchange, nf, nt), out_shape=(*outs(lamb...  79 us
    pallas_call x1, Pallas kernels, finish(): pl.pallas_call(functools.partial(apply, nf, nt), in_specs=[vmem] * 13, ou...  4.78 us

profile of v1, /device:TPU:0, one launch (start us, length us, event | category | flops | bytes accessed | tf_op | source)
XLA Modules:
  0.0 84.4 jit_solution(6401509344779746129)
XLA Ops:
  0.6 79.0 %exchange.1 = (bf16[8,256,1024]{2,1,0:T(8,128)(2,1)S(1)}, bf16[8,128,512]{2,1,0:T(8,128)(2,1)S(1)}, bf16[8,256,256]{2,1,0:T(8,128)(2,1)S(1)}, bf16[8,128,256]{2,...) custom-call(bf16[1536,512]{1,0:T(8,128)(2,1)} %refs_0_.1, ...), custom_call_target="tpu_custom_call" | custom-call | tf_op jit(solution)/shard_map/exchange/pallas_call | solution.py:425
  79.7 4.8 %apply.1 = (f32[256,1024]{1,0:T(8,128)}, f32[256,1024]{1,0:T(8,128)}, bf16[2048,1024]{1,0:T(8,128)(2,1)}, f32[256,1024]{1,0:T(8,128)}, f32[256,1024]{1,0:T(8,128...) custom-call(bf16[8,256,1024]{2,1,0:T(8,128)(2,1)S(1)} %get-tuple-ele, ...), custom_call_target="tpu_custom_call" | custom-call | tf_op jit(solution)/shard_map/apply/pallas_call | solution.py:505

commit v2 on v1

v2 whole, which is shorter than its diff:
```python
import functools

import jax
import jax.numpy as jnp
from jax import lax
from jax.experimental import pallas as pl
from jax.experimental.pallas import tpu as pltpu
from jax.sharding import PartitionSpec as P

LEARN_RATE = 0.01
MEAN_DECAY = 0.8
BETA_SQUARE = 0.9
EPS_RMS = 1e-06
MESH = pl.DeviceIdType.MESH
F32, BF16 = jnp.float32, jnp.bfloat16
PAIR = (0, 1)
CORES = 2
NEAR = (((1, 0), (1, 1)), ((1, 2),), ((1, 3), (1, 4)), ((2, 0),), ((2, 1),), ((2, 2),), ((2, 3),), ((2, 4),))


def rcopy(src, dst, send, recv, fs, tp):
    return pltpu.make_async_remote_copy(
        src_ref=src, dst_ref=dst, send_sem=send, recv_sem=recv,
        device_id=(fs, tp), device_id_type=MESH,
    )


def over_rows(left, right):
    return lax.dot_general(left, right, (((0,), (0,)), ((), ())), preferred_element_type=F32)


def unit_heights(heights, widths):
    least = min(h * w for h, w in zip(heights, widths))
    return [least // w for w in widths]


def parts_of(height, nt):
    return min(nt, height // 16)


def exchange(nf, nt, *refs):
    hbm, rest = refs[:12], refs[12:]
    wg, bg, dirs, mean_new, square_new, w32 = (rest[2 * k:2 * k + 2] for k in range(6))
    totals, rest = rest[12], rest[13:]
    left, right, mean, square = (rest[2 * k:2 * k + 2] for k in range(4))
    sbuf, rbuf, kept, lifted, part, psend, pbuf, zsend, zbuf, tot = (rest[8 + 4 * k:12 + 4 * k] for k in range(10))
    (tsend, tbuf, isem, b_s, b_r, bd_s, bd_r, c_s, c_r, e_s, e_r, cd_s, cd_r, w_u, w_d, w_r, wd_s, wd_r,
     rs_s, rs_r, ag_s, ag_r, p_s, p_r, z_s, z_r, g_s, g_r, gd_s, gd_r, t_s, t_r) = rest[48:]

    nz = nf // CORES
    f, t = lax.axis_index("fs"), lax.axis_index("tp")
    z, c = lax.div(f, CORES), lax.rem(f, CORES)
    partner = f + 1 - 2 * c
    rank = bg[0].shape[2]
    half = rank // 2
    tokens = left[0].shape[0]
    peers_t = [lax.rem(t + s, nt) for s in range(1, nt)]
    peers_z = [lax.rem(z + s, nz) for s in range(1, nz)]
    own_column = z == t
    elsewhere = jnp.logical_not(own_column)

    held = (*left, *right, *w32, *[b.at[f] for b in bg], *mean, *square)
    order = (6, 7, 4, 5, 0, 1, 2, 3, 8, 9, 10, 11)
    fetch = [pltpu.make_async_copy(hbm[k], held[k], isem.at[k]) for k in range(12)]
    for k in order:
        fetch[k].start()

    barrier = pltpu.get_barrier_semaphore()
    pl.semaphore_signal(barrier, inc=1, device_id=(partner, t), device_id_type=MESH)
    for pz in peers_z:
        pl.semaphore_signal(barrier, inc=1, device_id=(pz * CORES + c, t), device_id_type=MESH)
    for pt in peers_t:
        pl.semaphore_signal(barrier, inc=1, device_id=(f, pt), device_id_type=MESH)
    pl.semaphore_wait(barrier, 1 + len(peers_z) + len(peers_t))

    lane = t * CORES + c
    other = t * CORES + 1 - c
    chunks = ((0, 0, half), (0, half, half), (1, 0, rank))

    def slab(i, block, column, first=0, size=rank):
        tall = bg[i].shape[1] // parts_of(bg[i].shape[1], nt)
        return bg[i].at[block, pl.ds(pl.multiple_of(column * tall, tall), tall), pl.ds(first, size)]

    def when_part(i, column, then):
        parts = parts_of(bg[i].shape[1], nt)
        if parts == nt:
            then()
        else:
            pl.when(column < parts)(then)

    def basis_line(k, pz, block):
        i, first, size = chunks[k]
        ref = slab(i, block, t, first, size)
        return rcopy(ref, ref, b_s.at[k, pz], b_r.at[k, lax.div(block, CORES)], pz * CORES + c, t)

    def basis_plane(k, b, column):
        i, first, size = chunks[k]
        ref = slab(i, b * CORES + c, column, first, size)
        return rcopy(ref, ref, c_s.at[k, b], c_r.at[k, column], f, b)

    def basis_core(k, block):
        i, first, size = chunks[k]
        ref = bg[i].at[block, :, pl.ds(first, size)]
        return rcopy(ref, ref, bd_s.at[k], bd_r.at[k], partner, t)

    def rest_plane(i, b, column, pt):
        ref = slab(i, b * CORES + c, column)
        return rcopy(ref, ref, e_s.at[i, b, pt], e_r.at[i, b, column], f, pt)

    def rest_core(i, block):
        ref = bg[i].at[block]
        return rcopy(ref, ref, cd_s.at[i, block], cd_r.at[i, block], partner, t)

    heights = [w.shape[1] for w in wg]
    tall = unit_heights(heights, [w.shape[2] for w in wg])
    units = [(i, r) for i in PAIR for r in range(0, heights[i], tall[i])]

    def unit(u, zb, core):
        i, r = units[u]
        return wg[i].at[zb * CORES + core, pl.ds(r, tall[i])]

    def w_up(u, zb):
        ref = unit(u, zb, c)
        return rcopy(ref, ref, w_u.at[u, zb], w_r.at[u, zb], f + CORES, t)

    def w_dn(u, zb):
        ref = unit(u, zb, c)
        return rcopy(ref, ref, w_d.at[u, zb], w_r.at[u, zb], f - CORES, t)

    def w_core(u, zb, core):
        ref = unit(u, zb, core)
        return rcopy(ref, ref, wd_s.at[u, zb], wd_r.at[u, zb], partner, t)

    def weights_on(events):
        for s, u in events:
            if s > nz - 1:
                continue

            @pl.when(z >= s)
            def _():
                w_up(u, z - s).wait_recv()

                @pl.when(z < nz - 1)
                def _():
                    w_up(u, z - s).start()
                w_core(u, z - s, c).start()

            @pl.when(z + s <= nz - 1)
            def _():
                w_dn(u, z + s).wait_recv()

                @pl.when(z > 0)
                def _():
                    w_dn(u, z + s).start()
                w_core(u, z + s, c).start()

    fetch[6].wait()
    fetch[7].wait()
    for k in range(len(chunks)):
        def to_line(k=k):
            for pz in [lax.rem(z + s, nz) for s in range(nz // 2, nz)] + [lax.rem(z + s, nz) for s in range(1, nz // 2)]:
                basis_line(k, pz, f).start()
        when_part(chunks[k][0], t, to_line)

    @pl.when(own_column)
    def _():
        for k in range(len(chunks)):
            basis_core(k, lane).start()
    for i in PAIR:
        fetch[4 + i].wait()
        wg[i][f] = w32[i][...].astype(BF16)
    for u in range(len(units)):
        @pl.when(z < nz - 1)
        def _():
            w_up(u, z).start()

        @pl.when(z > 0)
        def _():
            w_dn(u, z).start()

    levels = nt.bit_length() - 1
    sizes = [tokens // 2 >> k for k in range(levels + 1)]
    offs = [sizes[0] - s for s in sizes]
    masks = [[1 << k for k in range(levels)], [1 << k for k in reversed(range(levels))]]
    bits = [[lax.rem(lax.div(t, m), 2) for m in masks[h]] for h in PAIR]
    mates = [[t + m * (1 - 2 * b) for m, b in zip(masks[h], bits[h])] for h in PAIR]
    bases = []
    for h in PAIR:
        at = [h * sizes[0]]
        for k in range(levels):
            at.append(at[-1] + bits[h][k] * sizes[k + 1])
        bases.append(at)
    streams = tuple((i, r) for i in PAIR for r in PAIR)

    def rows(start, size):
        return pl.ds(pl.multiple_of(start, 16), size)

    def away(h, k):
        return rows(bases[h][k] + (1 - bits[h][k]) * sizes[k + 1], sizes[k + 1])

    def rs(q, h, k):
        at = pl.ds(offs[k], sizes[k + 1])
        return rcopy(sbuf[q].at[h, at], rbuf[q].at[h, at], rs_s.at[q, h, k], rs_r.at[q, h, k], f, mates[h][k])

    def ag(q, h, k, received=False):
        ref = lifted[q].at[away(h, k) if received else rows(bases[h][k + 1], sizes[k + 1])]
        return rcopy(ref, ref, ag_s.at[q, h, k], ag_r.at[q, h, k], f, mates[h][k])

    def basis_in(k):
        def from_line():
            for b in peers_z:
                basis_line(k, b, b * CORES + c).wait_recv()

                @pl.when(b != t)
                def _():
                    basis_plane(k, b, t).start()

        when_part(chunks[k][0], t, from_line)

    def basis_joined(k):
        @pl.when(elsewhere)
        def _():
            for pt in peers_t:
                when_part(chunks[k][0], pt, lambda: basis_plane(k, t, pt).wait_recv())
            basis_core(k, lane).start()

    def lift(q):
        i, r = streams[q]
        two = bg[i][pl.ds(t * CORES, CORES), :, r * half:(r + 1) * half]
        factor = two.reshape(two.shape[0] * two.shape[1], half)
        for h in PAIR:
            sbuf[q][h, pl.ds(0, sizes[1])] = jnp.dot(
                left[i][away(h, 0), :], factor, preferred_element_type=F32).astype(BF16)
            rs(q, h, 0).start()
        for h in PAIR:
            kept[q][h, pl.ds(0, sizes[1])] = jnp.dot(
                left[i][rows(bases[h][1], sizes[1]), :], factor, preferred_element_type=F32)

    def contract(q, at, first=False):
        i = streams[q][0]
        got = over_rows(lifted[q][at, :], right[i][at, :]).reshape(part[q].shape)
        if first:
            part[q][...] = got
        else:
            part[q][...] += got

    def halve(q, k):
        for h in PAIR:
            rs(q, h, k).wait_recv()
            if k + 1 < levels:
                small = sizes[k + 2]
                for b, mine in ((1 - bits[h][k + 1], False), (bits[h][k + 1], True)):
                    at = rows(offs[k] + b * small, small)
                    both = kept[q][h, at] + rbuf[q][h, at].astype(F32)
                    to = pl.ds(offs[k + 1], small)
                    if mine:
                        kept[q][h, to] = both
                    else:
                        sbuf[q][h, to] = both.astype(BF16)
                        rs(q, h, k + 1).start()
            else:
                at = pl.ds(offs[k], sizes[k + 1])
                lifted[q][rows(bases[h][k + 1], sizes[k + 1]), :] = (
                    kept[q][h, at] + rbuf[q][h, at].astype(F32)).astype(BF16)
                ag(q, h, k).start()
        if k + 1 == levels:
            i, r = streams[q]
            if r == 0:
                fetch[2 + i].wait()
            for h in PAIR:
                contract(q, rows(bases[h][levels], sizes[levels]), h == 0)

    def double(q, k):
        for h in PAIR:
            ag(q, h, k, True).wait_recv()
            if k > 0:
                ag(q, h, k - 1).start()
        for h in PAIR:
            contract(q, away(h, k))

    pairs = [rcopy(psend[q], pbuf[q], p_s.at[q], p_r.at[q], partner, t) for q in range(4)]
    me = c * nz + z

    def line(q, pz):
        return rcopy(zsend[q].at[pz], zbuf[q].at[z], z_s.at[q, pz], z_r.at[q, z], pz * CORES + c, t)

    def line_got(q, pz):
        return rcopy(zsend[q].at[pz], zbuf[q].at[pz], z_s.at[q, pz], z_r.at[q, pz], pz * CORES + c, t)

    def share(q, pz, at):
        ref = tot[q].at[at]
        return rcopy(ref, ref, g_s.at[q, pz], g_r.at[q, at - c * nz], pz * CORES + c, t)

    def share_core(q, core, zz):
        ref = tot[q].at[core * nz + zz]
        return rcopy(ref, ref, gd_s.at[q, zz], gd_r.at[q, zz], partner, t)

    def pair_send(q):
        for zz in range(nz):
            psend[q][zz] = part[q][(1 - c) * nz + zz].astype(BF16)
        pairs[q].start()

    def line_send(q):
        pairs[q].wait_recv()
        for pz in peers_z:
            zsend[q][pz] = (part[q][c * nz + pz] + pbuf[q][pz].astype(F32)).astype(BF16)
            line(q, pz).start()

    def line_sum(q):
        acc = part[q][me] + pbuf[q][z].astype(F32)
        for pz in peers_z:
            line_got(q, pz).wait_recv()
            acc = acc + zbuf[q][pz].astype(F32)
        tot[q][me] = acc.astype(BF16)
        for pz in peers_z:
            share(q, pz, me).start()
        share_core(q, c, z).start()

    def line_take(q):
        for pz in peers_z:
            share(q, pz, c * nz + pz).wait_recv()
            share_core(q, c, pz).start()

    def direct(q):
        i, r = streams[q]
        if r == 0:
            fetch[8 + i].wait()
            fetch[10 + i].wait()
        for zz in range(nz):
            share_core(q, 1 - c, zz).wait_recv()
        at = pl.ds(r * half, half)
        proj = tot[q][...].astype(F32).reshape(half, tot[q].shape[2])
        mean_out = MEAN_DECAY * mean[i][at, :] + (1.0 - MEAN_DECAY) * proj
        square_out = BETA_SQUARE * square[i][at, :] + (1.0 - BETA_SQUARE) * proj * proj
        mean_new[i][at, :] = mean_out
        square_new[i][at, :] = square_out
        dirs[i][at, :] = (mean_out / jnp.sqrt(square_out)).astype(BF16)

    def norm(i):
        height = bg[i].shape[1]
        group = max(1, 1024 // height)
        sums = jnp.zeros((1, dirs[i].shape[1]), F32)
        for g in range(0, nf, group):
            some = bg[i][g:g + group]
            u = jnp.dot(some.reshape(some.shape[0] * height, rank), dirs[i][...], preferred_element_type=F32)
            sums = sums + jnp.sum(u * u, axis=0, keepdims=True)
        tile = jnp.zeros((8, 128), F32) + jnp.sum(sums, axis=1, keepdims=True)
        tsend[i] = tile
        tbuf[t, i] = tile

    def rest_send(i):
        def parts():
            for b in peers_z:
                for pt in peers_t:
                    @pl.when(pt != b)
                    def _():
                        rest_plane(i, b, t, pt).start()
        when_part(i, t, parts)

        @pl.when(elsewhere)
        def _():
            rest_core(i, f).start()

    def rest_take(i):
        for b in peers_z:
            @pl.when(b != t)
            def _():
                for pt in peers_t:
                    when_part(i, pt, lambda: rest_plane(i, b, pt, pt).wait_recv())
                rest_core(i, b * CORES + c).start()

    def rest_end(i):
        for pt in peers_t:
            rest_core(i, pt * CORES + 1 - c).wait_recv()

    for k in range(len(chunks)):
        basis_in(k)
    for k in range(len(chunks)):
        basis_joined(k)
    fetch[0].wait()
    basis_core(0, other).wait_recv()
    lift(0)
    basis_core(1, other).wait_recv()
    lift(1)
    for u in range(len(units)):
        w_core(u, z, c).start()
    fetch[1].wait()
    basis_core(2, other).wait_recv()
    halve(0, 0)
    lift(2)
    weights_on(NEAR[0])
    halve(1, 0)
    for k in range(1, levels - 1):
        for q in PAIR:
            halve(q, k)
    halve(0, levels - 1)
    lift(3)
    weights_on(NEAR[1])
    halve(1, levels - 1)
    for k in range(levels - 1, 0, -1):
        for q in PAIR:
            double(q, k)
    weights_on(NEAR[2])
    halve(2, 0)
    double(0, 0)
    pair_send(0)
    halve(3, 0)
    double(1, 0)
    pair_send(1)
    for k in range(1, levels - 1):
        for q in (2, 3):
            halve(q, k)
    line_send(0)
    halve(2, levels - 1)
    line_send(1)
    halve(3, levels - 1)
    weights_on(NEAR[3])
    for k in range(levels - 1, 0, -1):
        for q in (2, 3):
            double(q, k)
    weights_on(NEAR[4])
    double(2, 0)
    pair_send(2)
    line_sum(0)
    double(3, 0)
    pair_send(3)
    for i in PAIR:
        rest_send(i)
    line_sum(1)
    line_send(2)
    line_send(3)
    weights_on(NEAR[5])
    line_take(0)
    line_take(1)
    for i in PAIR:
        rest_take(i)
    line_sum(2)
    line_sum(3)
    weights_on(NEAR[6])
    direct(0)
    direct(1)
    for i in PAIR:
        rest_end(i)
    norm(0)
    line_take(2)
    line_take(3)
    weights_on(NEAR[7])
    direct(2)
    direct(3)
    norm(1)
    for pt in peers_t:
        rcopy(tsend, tbuf.at[t], t_s.at[pt], t_r.at[t], f, pt).start()
    weights_on([(s, u) for s in range(3, nz) for u in range(len(units))])

    for pt in peers_t:
        rcopy(tsend, tbuf.at[pt], t_s.at[pt], t_r.at[pt], f, pt).wait_recv()
    summed = tbuf[0]
    for k in range(1, nt):
        summed = summed + tbuf[k]
    totals[...] = summed

    for u in range(len(units)):
        for zb in range(nz):
            w_core(u, zb, 1 - c).wait_recv()
    for k in range(len(chunks)):
        def line_out(k=k):
            for pz in peers_z:
                basis_line(k, pz, f).wait_send()

                @pl.when(pz != t)
                def _():
                    basis_plane(k, pz, t).wait_send()
        when_part(chunks[k][0], t, line_out)
        basis_core(k, lane).wait_send()
    for i in PAIR:
        def rest_out(i=i):
            for b in peers_z:
                for pt in peers_t:
                    @pl.when(pt != b)
                    def _():
                        rest_plane(i, b, t, pt).wait_send()
        when_part(i, t, rest_out)

        @pl.when(elsewhere)
        def _():
            rest_core(i, f).wait_send()
        for b in peers_z:
            @pl.when(b != t)
            def _():
                rest_core(i, b * CORES + c).wait_send()
    for q in range(4):
        for h in PAIR:
            for k in range(levels):
                rs(q, h, k).wait_send()
                ag(q, h, k).wait_send()
        pairs[q].wait_send()
        for pz in peers_z:
            line(q, pz).wait_send()
            share(q, pz, me).wait_send()
        for zz in range(nz):
            share_core(q, c, zz).wait_send()
    for u in range(len(units)):
        for zb in range(nz):
            w_core(u, zb, c).wait_send()

            @pl.when((z >= zb) & (z < nz - 1))
            def _():
                w_up(u, zb).wait_send()

            @pl.when((z <= zb) & (z > 0))
            def _():
                w_dn(u, zb).wait_send()
    for pt in peers_t:
        rcopy(tsend, tbuf.at[t], t_s.at[pt], t_r.at[t], f, pt).wait_send()


def gather_and_reduce(nf, nt, lefts, rights, weights, bases, means, squares):
    rank, nz, tokens = bases[0].shape[1], nf // CORES, rights[0].shape[0]
    half, levels = rank // 2, nt.bit_length() - 1
    seg = half // nf
    heights, widths = [b.shape[0] for b in bases], [r.shape[1] for r in rights]
    units = sum(h // u for h, u in zip(heights, unit_heights(heights, widths)))
    vmem, dma = pl.BlockSpec(memory_space=pltpu.VMEM), pltpu.SemaphoreType.DMA
    hbm = pl.BlockSpec(memory_space=pltpu.HBM)

    def two(shape_of, kind=BF16, make=pltpu.VMEM):
        return [make(shape_of(h, w), kind) for h, w in zip(heights, widths)]

    def four(shape_of, kind=BF16):
        return [pltpu.VMEM(shape_of(w), kind) for w in widths for _ in PAIR]

    def outs(shape_of, kind=BF16):
        return two(shape_of, kind, jax.ShapeDtypeStruct)

    halves = lambda w: (2, tokens // 2, half)
    pieces = lambda w: (nz, seg, w)
    ranked = lambda h, w: (rank, w)
    fetched = (*lefts, *rights, *means, *squares)
    return pl.pallas_call(
        functools.partial(exchange, nf, nt),
        out_shape=(
            *outs(lambda h, w: (nf, h, w)), *outs(lambda h, w: (nf, h, rank)), *outs(ranked),
            *outs(ranked, F32), *outs(ranked, F32), *outs(lambda h, w: (h, w), F32),
            jax.ShapeDtypeStruct((2, 8, 128), F32),
        ),
        in_specs=[hbm] * 12,
        out_specs=(vmem,) * 13,
        scratch_shapes=[
            *[pltpu.VMEM(x.shape, x.dtype) for x in fetched],
            *four(halves), *four(halves), *four(halves, F32), *four(lambda w: (tokens, half)),
            *four(lambda w: (nf, seg, w), F32), *four(pieces), *four(pieces), *four(pieces), *four(pieces),
            *four(lambda w: (nf, seg, w)),
            pltpu.VMEM((2, 8, 128), F32),
            pltpu.VMEM((nt, 2, 8, 128), F32),
            dma((12,)), dma((3, nz)), dma((3, nz)), dma((3,)), dma((3,)),
            dma((3, nz)), dma((3, nt)), dma((2, nz, nt)), dma((2, nz, nt)), dma((2, nf)), dma((2, nf)),
            *[dma((units, nz))] * 5,
            *[dma((4, 2, levels))] * 4,
            dma((4,)), dma((4,)), *[dma((4, nz))] * 6, dma((nt,)), dma((nt,)),
        ],
        compiler_params=pltpu.CompilerParams(
            collective_id=0, has_side_effects=True, vmem_limit_bytes=40 * 1024 * 1024
        ),
        name="exchange",
    )(*[pltpu.with_memory_space_constraint(x, pltpu.HBM)
        for x in (*lefts, *rights, *weights, *bases, *means, *squares)])


def apply(nf, nt, *refs):
    wg, bg, dirs, mean_new, square_new, w32 = (refs[2 * k:2 * k + 2] for k in range(6))
    totals = refs[12]
    outs = [refs[13 + 5 * i:18 + 5 * i] for i in PAIR]
    step, new, copy = (refs[23 + 2 * k:25 + 2 * k] for k in range(3))
    sem, csem = refs[29:]
    f = lax.axis_index("fs")

    def to(k, i):
        src = (step, new, None, mean_new, square_new)[k]
        return pltpu.make_async_copy(src[i], outs[i][k], sem.at[i, k])

    def block(i, g):
        height = w32[i].shape[0]
        return pltpu.make_async_copy(copy[i].at[pl.ds(g * height, height)],
                                     outs[i][2].at[pl.ds(g * height, height)], csem.at[i, g])

    for i in PAIR:
        to(3, i).start()
        to(4, i).start()
    scales = []
    for i in PAIR:
        count = w32[i].shape[0] * nf * w32[i].shape[1] * nt
        scale = LEARN_RATE * lax.rsqrt(totals[i, 0:1, 0:1] / lax.convert_element_type(count, F32) + EPS_RMS)
        scales.append(scale)
        own = scale * jnp.dot(bg[i][f], dirs[i][...], preferred_element_type=F32)
        step[i][...] = own
        new[i][...] = w32[i][...] - own
        to(0, i).start()
        to(1, i).start()
    for i in PAIR:
        height = w32[i].shape[0]
        for g in range(nf):
            update = jnp.dot(bg[i][g], dirs[i][...], preferred_element_type=F32)
            copy[i][pl.ds(g * height, height), :] = (wg[i][g].astype(F32) - scales[i] * update).astype(BF16)
            block(i, g).start()
    for i in PAIR:
        for k in (0, 1, 3, 4):
            to(k, i).wait()
        for g in range(nf):
            block(i, g).wait()


def finish(nf, nt, gathered):
    w32 = gathered[10:12]
    vmem, hbm = pl.BlockSpec(memory_space=pltpu.VMEM), pl.BlockSpec(memory_space=pltpu.HBM)
    out_shape = []
    for i in PAIR:
        copy = jax.ShapeDtypeStruct((nf * w32[i].shape[0], w32[i].shape[1]), BF16)
        like = lambda x: jax.ShapeDtypeStruct(x.shape, F32)
        out_shape += [like(w32[i]), like(w32[i]), copy, like(gathered[6 + i]), like(gathered[8 + i])]
    return pl.pallas_call(
        functools.partial(apply, nf, nt),
        in_specs=[vmem] * 13,
        out_specs=[hbm] * 10,
        out_shape=out_shape,
        scratch_shapes=[
            *[pltpu.VMEM(w.shape, F32) for w in w32], *[pltpu.VMEM(w.shape, F32) for w in w32],
            *[pltpu.VMEM(out_shape[2 + 5 * i].shape, BF16) for i in PAIR],
            pltpu.SemaphoreType.DMA((2, 5)), pltpu.SemaphoreType.DMA((2, nf)),
        ],
        compiler_params=pltpu.CompilerParams(vmem_limit_bytes=12 * 1024 * 1024),
        name="apply",
    )(*gathered)


def per_device(nf, nt, attn_out, out_cot, latent, value_cot, out_weight, value_up_matrix,
               out_basis, value_basis, out_mean, out_square, value_mean, value_square):
    gathered = gather_and_reduce(
        nf, nt, (attn_out, latent), (out_cot, value_cot), (out_weight, value_up_matrix),
        (out_basis, value_basis), (out_mean, value_mean), (out_square, value_square))
    return tuple(finish(nf, nt, gathered))


def solution(mesh):
    both, rows, cols = P("fs", "tp"), P("fs", None), P(None, "tp")
    return jax.shard_map(
        functools.partial(per_device, mesh.shape["fs"], mesh.shape["tp"]),
        mesh=mesh,
        in_specs=(both,) * 6 + (rows,) * 2 + (cols,) * 4,
        out_specs=(both, both, cols, cols, cols) * 2,
        check_vma=False,
    )
```

time: 84.6 us -> 74.7 us (0.88)
  Pallas kernels: 83.8 us -> 73.9 us
    pallas_call x1, Pallas kernels: 79 us -> 69.2 us  [gather_and_reduce(): pl.pallas_call(functools.partial(exchange, nf, nt), out_shape=(*outs(lamb...]
where the time goes in v2:
time: 74.7 us; the launch traced here: 74.6 us
  Pallas kernels  73.9 us (99%)
    pallas_call x1, Pallas kernels, gather_and_reduce(): pl.pallas_call(functools.partial(exchange, nf, nt), out_shape=(*outs(lamb...  69.2 us
    pallas_call x1, Pallas kernels, finish(): pl.pallas_call(functools.partial(apply, nf, nt), in_specs=[vmem] * 13, ou...  4.78 us

profile of v2, /device:TPU:0, one launch (start us, length us, event | category | flops | bytes accessed | tf_op | source)
XLA Modules:
  0.0 74.6 jit_solution(3528751767218958823)
XLA Ops:
  0.6 69.2 %exchange.1 = (bf16[8,256,1024]{2,1,0:T(8,128)(2,1)S(1)}, bf16[8,128,512]{2,1,0:T(8,128)(2,1)S(1)}, bf16[8,256,256]{2,1,0:T(8,128)(2,1)S(1)}, bf16[8,128,256]{2,...) custom-call(bf16[1536,512]{1,0:T(8,128)(2,1)} %refs_0_.1, ...), custom_call_target="tpu_custom_call" | custom-call | tf_op jit(solution)/shard_map/exchange/pallas_call | solution.py:539
  69.8 4.8 %apply.1 = (f32[256,1024]{1,0:T(8,128)}, f32[256,1024]{1,0:T(8,128)}, bf16[2048,1024]{1,0:T(8,128)(2,1)}, f32[256,1024]{1,0:T(8,128)}, f32[256,1024]{1,0:T(8,128...) custom-call(bf16[8,256,1024]{2,1,0:T(8,128)(2,1)S(1)} %get-tuple-ele, ...), custom_call_target="tpu_custom_call" | custom-call | tf_op jit(solution)/shard_map/apply/pallas_call | solution.py:620

commit v3 on v2

--- a/solution.py
+++ b/solution.py
@@ -15,7 +15,7 @@
 F32, BF16 = jnp.float32, jnp.bfloat16
 PAIR = (0, 1)
 CORES = 2
-NEAR = (((1, 0), (1, 1)), ((1, 2),), ((1, 3), (1, 4)), ((2, 0),), ((2, 1),), ((2, 2),), ((2, 3),), ((2, 4),))
+NEAR = (((1, 0), (1, 1)), ((1, 2), (1, 3)), ((1, 4), (2, 0)), ((2, 1),), ((2, 2),), ((2, 3),), ((2, 4),))
 
 
 def rcopy(src, dst, send, recv, fs, tp):
@@ -40,12 +40,12 @@
 
 def exchange(nf, nt, *refs):
     hbm, rest = refs[:12], refs[12:]
-    wg, bg, dirs, mean_new, square_new, w32 = (rest[2 * k:2 * k + 2] for k in range(6))
-    totals, rest = rest[12], rest[13:]
-    left, right, mean, square = (rest[2 * k:2 * k + 2] for k in range(4))
-    sbuf, rbuf, kept, lifted, part, psend, pbuf, zsend, zbuf, tot = (rest[8 + 4 * k:12 + 4 * k] for k in range(10))
+    wg, full, mean_new, square_new, w32 = (rest[2 * k:2 * k + 2] for k in range(5))
+    totals, rest = rest[10], rest[11:]
+    left, right, mean, square, bg, dirs = (rest[2 * k:2 * k + 2] for k in range(6))
+    sbuf, rbuf, kept, lifted, part, psend, pbuf, zsend, zbuf, tot = (rest[12 + 4 * k:16 + 4 * k] for k in range(10))
     (tsend, tbuf, isem, b_s, b_r, bd_s, bd_r, c_s, c_r, e_s, e_r, cd_s, cd_r, w_u, w_d, w_r, wd_s, wd_r,
-     rs_s, rs_r, ag_s, ag_r, p_s, p_r, z_s, z_r, g_s, g_r, gd_s, gd_r, t_s, t_r) = rest[48:]
+     rs_s, rs_r, ag_s, ag_r, p_s, p_r, z_s, z_r, g_s, g_r, gd_s, gd_r, t_s, t_r) = rest[52:]
 
     nz = nf // CORES
     f, t = lax.axis_index("fs"), lax.axis_index("tp")
@@ -73,6 +73,15 @@
         pl.semaphore_signal(barrier, inc=1, device_id=(f, pt), device_id_type=MESH)
     pl.semaphore_wait(barrier, 1 + len(peers_z) + len(peers_t))
 
+    def took(ref, sem):
+        pltpu.make_async_copy(ref, ref, sem).wait()
+
+    def took_slabs(k_or_i, sem, count, first=0, size=None):
+        size = rank if size is None else size
+        i = k_or_i
+        tall = bg[i].shape[1] // parts_of(bg[i].shape[1], nt)
+        took(lifted[0].at[pl.ds(0, count * tall * size // half)], sem)
+
     lane = t * CORES + c
     other = t * CORES + 1 - c
     chunks = ((0, 0, half), (0, half, half), (1, 0, rank))
@@ -91,12 +100,12 @@
     def basis_line(k, pz, block):
         i, first, size = chunks[k]
         ref = slab(i, block, t, first, size)
-        return rcopy(ref, ref, b_s.at[k, pz], b_r.at[k, lax.div(block, CORES)], pz * CORES + c, t)
+        return rcopy(ref, ref, b_s.at[k], b_r.at[k], pz * CORES + c, t)
 
     def basis_plane(k, b, column):
         i, first, size = chunks[k]
         ref = slab(i, b * CORES + c, column, first, size)
-        return rcopy(ref, ref, c_s.at[k, b], c_r.at[k, column], f, b)
+        return rcopy(ref, ref, c_s.at[k], c_r.at[k], f, b)
 
     def basis_core(k, block):
         i, first, size = chunks[k]
@@ -105,11 +114,11 @@
 
     def rest_plane(i, b, column, pt):
         ref = slab(i, b * CORES + c, column)
-        return rcopy(ref, ref, e_s.at[i, b, pt], e_r.at[i, b, column], f, pt)
+        return rcopy(ref, ref, e_s.at[i, b], e_r.at[i, b], f, pt)
 
     def rest_core(i, block):
         ref = bg[i].at[block]
-        return rcopy(ref, ref, cd_s.at[i, block], cd_r.at[i, block], partner, t)
+        return rcopy(ref, ref, cd_s.at[i], cd_r.at[i], partner, t)
 
     heights = [w.shape[1] for w in wg]
     tall = unit_heights(heights, [w.shape[2] for w in wg])
@@ -121,15 +130,15 @@
 
     def w_up(u, zb):
         ref = unit(u, zb, c)
-        return rcopy(ref, ref, w_u.at[u, zb], w_r.at[u, zb], f + CORES, t)
+        return rcopy(ref, ref, w_u.at[units[u][0]], w_r.at[u, zb], f + CORES, t)
 
     def w_dn(u, zb):
         ref = unit(u, zb, c)
-        return rcopy(ref, ref, w_d.at[u, zb], w_r.at[u, zb], f - CORES, t)
+        return rcopy(ref, ref, w_d.at[units[u][0]], w_r.at[u, zb], f - CORES, t)
 
     def w_core(u, zb, core):
         ref = unit(u, zb, core)
-        return rcopy(ref, ref, wd_s.at[u, zb], wd_r.at[u, zb], partner, t)
+        return rcopy(ref, ref, wd_s.at[units[u][0]], wd_r.at[units[u][0]], partner, t)
 
     def weights_on(events):
         for s, u in events:
@@ -200,28 +209,38 @@
 
     def rs(q, h, k):
         at = pl.ds(offs[k], sizes[k + 1])
-        return rcopy(sbuf[q].at[h, at], rbuf[q].at[h, at], rs_s.at[q, h, k], rs_r.at[q, h, k], f, mates[h][k])
-
-    def ag(q, h, k, received=False):
-        ref = lifted[q].at[away(h, k) if received else rows(bases[h][k + 1], sizes[k + 1])]
-        return rcopy(ref, ref, ag_s.at[q, h, k], ag_r.at[q, h, k], f, mates[h][k])
+        return rcopy(sbuf[q].at[h, at], rbuf[q].at[h, at], rs_s.at[q], rs_r.at[q, k], f, mates[h][k])
+
+    def ag(q, h, k):
+        ref = lifted[q].at[rows(bases[h][k + 1], sizes[k + 1])]
+        return rcopy(ref, ref, ag_s.at[q], ag_r.at[q, k], f, mates[h][k])
+
+    def senders(i, then):
+        parts = parts_of(bg[i].shape[1], nt)
+        if parts == nt:
+            then(nt - 1)
+        else:
+            pl.when(t < parts)(lambda: then(parts - 1))
+            pl.when(t >= parts)(lambda: then(parts))
 
     def basis_in(k):
+        i, first, size = chunks[k]
+
         def from_line():
+            took_slabs(i, b_r.at[k], nz - 1, size=size)
             for b in peers_z:
-                basis_line(k, b, b * CORES + c).wait_recv()
-
                 @pl.when(b != t)
                 def _():
                     basis_plane(k, b, t).start()
 
-        when_part(chunks[k][0], t, from_line)
+        when_part(i, t, from_line)
 
     def basis_joined(k):
+        i, first, size = chunks[k]
+
         @pl.when(elsewhere)
         def _():
-            for pt in peers_t:
-                when_part(chunks[k][0], pt, lambda: basis_plane(k, t, pt).wait_recv())
+            senders(i, lambda n: took_slabs(i, c_r.at[k], n, size=size))
             basis_core(k, lane).start()
 
     def lift(q):
@@ -245,8 +264,8 @@
             part[q][...] += got
 
     def halve(q, k):
+        took(rbuf[q].at[:, pl.ds(offs[k], sizes[k + 1])], rs_r.at[q, k])
         for h in PAIR:
-            rs(q, h, k).wait_recv()
             if k + 1 < levels:
                 small = sizes[k + 2]
                 for b, mine in ((1 - bits[h][k + 1], False), (bits[h][k + 1], True)):
@@ -271,9 +290,9 @@
                 contract(q, rows(bases[h][levels], sizes[levels]), h == 0)
 
     def double(q, k):
-        for h in PAIR:
-            ag(q, h, k, True).wait_recv()
-            if k > 0:
+        took(lifted[q].at[pl.ds(0, 2 * sizes[k + 1])], ag_r.at[q, k])
+        if k > 0:
+            for h in PAIR:
                 ag(q, h, k - 1).start()
         for h in PAIR:
             contract(q, away(h, k))
@@ -281,19 +300,36 @@
     pairs = [rcopy(psend[q], pbuf[q], p_s.at[q], p_r.at[q], partner, t) for q in range(4)]
     me = c * nz + z
 
+    chained = (0, 1)
+
     def line(q, pz):
-        return rcopy(zsend[q].at[pz], zbuf[q].at[z], z_s.at[q, pz], z_r.at[q, z], pz * CORES + c, t)
-
-    def line_got(q, pz):
-        return rcopy(zsend[q].at[pz], zbuf[q].at[pz], z_s.at[q, pz], z_r.at[q, pz], pz * CORES + c, t)
+        return rcopy(zsend[q].at[pz], zbuf[q].at[z], z_s.at[q], z_r.at[q, 0], pz * CORES + c, t)
+
+    def hop(q, zz, up, slot):
+        return rcopy(zsend[q].at[zz], zbuf[q].at[slot], z_s.at[q], z_r.at[q, 0 if up else 1],
+                     f + (CORES if up else -CORES), t)
+
+    def line_step(q, k):
+        for at, up in ((k, True), (nz - 1 - k, False)):
+            @pl.when(z == at)
+            def _():
+                if k > 0:
+                    took(zbuf[q].at[pl.ds(0, nz - k)], z_r.at[q, 0 if up else 1])
+                for zz in (range(at + 1, nz) if up else range(at)):
+                    sums = part[q][c * nz + zz] + pbuf[q][zz].astype(F32)
+                    if k > 0:
+                        sums = sums + zbuf[q][zz].astype(F32)
+                    zsend[q][zz] = sums.astype(BF16)
+                    beside = at + 1 if up else at - 1
+                    hop(q, zz, up, nz if zz == beside and not up else zz).start()
 
     def share(q, pz, at):
         ref = tot[q].at[at]
-        return rcopy(ref, ref, g_s.at[q, pz], g_r.at[q, at - c * nz], pz * CORES + c, t)
-
-    def share_core(q, core, zz):
-        ref = tot[q].at[core * nz + zz]
-        return rcopy(ref, ref, gd_s.at[q, zz], gd_r.at[q, zz], partner, t)
+        return rcopy(ref, ref, g_s.at[q], g_r.at[q], pz * CORES + c, t)
+
+    def share_core(q):
+        ref = tot[q].at[pl.ds(c * nz, nz)]
+        return rcopy(ref, ref, gd_s.at[q], gd_r.at[q], partner, t)
 
     def pair_send(q):
         for zz in range(nz):
@@ -302,32 +338,47 @@
 
     def line_send(q):
         pairs[q].wait_recv()
+        if q in chained:
+            line_step(q, 0)
+            return
         for pz in peers_z:
             zsend[q][pz] = (part[q][c * nz + pz] + pbuf[q][pz].astype(F32)).astype(BF16)
             line(q, pz).start()
 
     def line_sum(q):
         acc = part[q][me] + pbuf[q][z].astype(F32)
-        for pz in peers_z:
-            line_got(q, pz).wait_recv()
-            acc = acc + zbuf[q][pz].astype(F32)
-        tot[q][me] = acc.astype(BF16)
+        if q in chained:
+            for at in range(nz):
+                @pl.when(z == at)
+                def _():
+                    sums = acc
+                    if at > 0:
+                        if at == nz - 1:
+                            took(zbuf[q].at[pl.ds(0, 1)], z_r.at[q, 0])
+                        sums = sums + zbuf[q][at].astype(F32)
+                    if at < nz - 1:
+                        if at == 0:
+                            took(zbuf[q].at[pl.ds(0, 1)], z_r.at[q, 1])
+                        sums = sums + zbuf[q][nz].astype(F32)
+                    tot[q][at + c * nz] = sums.astype(BF16)
+        else:
+            took(zbuf[q].at[pl.ds(0, nz - 1)], z_r.at[q, 0])
+            for pz in peers_z:
+                acc = acc + zbuf[q][pz].astype(F32)
+            tot[q][me] = acc.astype(BF16)
         for pz in peers_z:
             share(q, pz, me).start()
-        share_core(q, c, z).start()
 
     def line_take(q):
-        for pz in peers_z:
-            share(q, pz, c * nz + pz).wait_recv()
-            share_core(q, c, pz).start()
+        took(tot[q].at[pl.ds(0, nz - 1)], g_r.at[q])
+        share_core(q).start()
 
     def direct(q):
         i, r = streams[q]
         if r == 0:
             fetch[8 + i].wait()
             fetch[10 + i].wait()
-        for zz in range(nz):
-            share_core(q, 1 - c, zz).wait_recv()
+        share_core(q).wait_recv()
         at = pl.ds(r * half, half)
         proj = tot[q][...].astype(F32).reshape(half, tot[q].shape[2])
         mean_out = MEAN_DECAY * mean[i][at, :] + (1.0 - MEAN_DECAY) * proj
@@ -343,6 +394,7 @@
         for g in range(0, nf, group):
             some = bg[i][g:g + group]
             u = jnp.dot(some.reshape(some.shape[0] * height, rank), dirs[i][...], preferred_element_type=F32)
+            full[i][g * height:(g + some.shape[0]) * height, :] = u
             sums = sums + jnp.sum(u * u, axis=0, keepdims=True)
         tile = jnp.zeros((8, 128), F32) + jnp.sum(sums, axis=1, keepdims=True)
         tsend[i] = tile
@@ -365,13 +417,51 @@
         for b in peers_z:
             @pl.when(b != t)
             def _():
-                for pt in peers_t:
-                    when_part(i, pt, lambda: rest_plane(i, b, pt, pt).wait_recv())
+                senders(i, lambda n: took_slabs(i, e_r.at[i, b], n))
                 rest_core(i, b * CORES + c).start()
 
     def rest_end(i):
-        for pt in peers_t:
-            rest_core(i, pt * CORES + 1 - c).wait_recv()
+        took(bg[i].at[pl.ds(0, nz - 1)], cd_r.at[i])
+
+    def basis_gone():
+        for k, (i, first, size) in enumerate(chunks):
+            def line_out(k=k, i=i, size=size):
+                took_slabs(i, b_s.at[k], nz - 1, size=size)
+                pl.when(elsewhere)(lambda: took_slabs(i, c_s.at[k], nz - 2, size=size))
+                pl.when(own_column)(lambda: took_slabs(i, c_s.at[k], nz - 1, size=size))
+            when_part(i, t, line_out)
+            basis_core(k, lane).wait_send()
+
+    def rest_gone():
+        for i in PAIR:
+            def rest_out(i=i):
+                for b in peers_z:
+                    pl.when(b == t)(lambda: took_slabs(i, e_s.at[i, b], nt - 1))
+                    pl.when(b != t)(lambda: took_slabs(i, e_s.at[i, b], nt - 2))
+            when_part(i, t, rest_out)
+            took(bg[i].at[pl.ds(0, nz - 1)], cd_s.at[i])
+
+    def tokens_gone(q):
+        sent = 2 * sum(sizes[1:])
+        took(lifted[q].at[pl.ds(0, sent)], rs_s.at[q])
+        took(lifted[q].at[pl.ds(0, sent)], ag_s.at[q])
+
+    def line_gone(q):
+        pairs[q].wait_send()
+        took(zsend[q].at[pl.ds(0, nz - 1)], z_s.at[q])
+        took(tot[q].at[pl.ds(0, nz - 1)], g_s.at[q])
+        share_core(q).wait_send()
+
+    def weights_gone():
+        for i in PAIR:
+            took(wg[i].at[pl.ds(0, nz)], wd_s.at[i])
+            for at in range(nz):
+                @pl.when(z == at)
+                def _():
+                    if at < nz - 1:
+                        took(wg[i].at[pl.ds(0, at + 1)], w_u.at[i])
+                    if at > 0:
+                        took(wg[i].at[pl.ds(0, nz - at)], w_d.at[i])
 
     for k in range(len(chunks)):
         basis_in(k)
@@ -418,25 +508,33 @@
     for k in range(levels - 1, 0, -1):
         for q in (2, 3):
             double(q, k)
+    line_step(0, 1)
+    line_step(1, 1)
     weights_on(NEAR[4])
     double(2, 0)
     pair_send(2)
-    line_sum(0)
+    for k in range(2, nz - 1):
+        line_step(0, k)
+        line_step(1, k)
     double(3, 0)
     pair_send(3)
-    for i in PAIR:
-        rest_send(i)
-    line_sum(1)
     line_send(2)
     line_send(3)
+    line_sum(0)
+    line_sum(1)
+    for i in PAIR:
+        rest_send(i)
     weights_on(NEAR[5])
-    line_take(0)
-    line_take(1)
-    for i in PAIR:
-        rest_take(i)
+    basis_gone()
+    tokens_gone(0)
+    tokens_gone(1)
     line_sum(2)
     line_sum(3)
     weights_on(NEAR[6])
+    line_take(0)
+    line_take(1)
+    for i in PAIR:
+        rest_take(i)
     direct(0)
     direct(1)
     for i in PAIR:
@@ -444,74 +542,26 @@
     norm(0)
     line_take(2)
     line_take(3)
-    weights_on(NEAR[7])
     direct(2)
     direct(3)
     norm(1)
     for pt in peers_t:
-        rcopy(tsend, tbuf.at[t], t_s.at[pt], t_r.at[t], f, pt).start()
+        rcopy(tsend, tbuf.at[t], t_s.at[0], t_r.at[0], f, pt).start()
+    rest_gone()
+    tokens_gone(2)
+    tokens_gone(3)
+    for q in range(4):
+        line_gone(q)
     weights_on([(s, u) for s in range(3, nz) for u in range(len(units))])
-
-    for pt in peers_t:
-        rcopy(tsend, tbuf.at[pt], t_s.at[pt], t_r.at[pt], f, pt).wait_recv()
+    took(tbuf.at[pl.ds(0, nt - 1)], t_r.at[0])
     summed = tbuf[0]
     for k in range(1, nt):
         summed = summed + tbuf[k]
     totals[...] = summed
-
-    for u in range(len(units)):
-        for zb in range(nz):
-            w_core(u, zb, 1 - c).wait_recv()
-    for k in range(len(chunks)):
-        def line_out(k=k):
-            for pz in peers_z:
-                basis_line(k, pz, f).wait_send()
-
-                @pl.when(pz != t)
-                def _():
-                    basis_plane(k, pz, t).wait_send()
-        when_part(chunks[k][0], t, line_out)
-        basis_core(k, lane).wait_send()
-    for i in PAIR:
-        def rest_out(i=i):
-            for b in peers_z:
-                for pt in peers_t:
-                    @pl.when(pt != b)
-                    def _():
-                        rest_plane(i, b, t, pt).wait_send()
-        when_part(i, t, rest_out)
-
-        @pl.when(elsewhere)
-        def _():
-            rest_core(i, f).wait_send()
-        for b in peers_z:
-            @pl.when(b != t)
-            def _():
-                rest_core(i, b * CORES + c).wait_send()
-    for q in range(4):
-        for h in PAIR:
-            for k in range(levels):
-                rs(q, h, k).wait_send()
-                ag(q, h, k).wait_send()
-        pairs[q].wait_send()
-        for pz in peers_z:
-            line(q, pz).wait_send()
-            share(q, pz, me).wait_send()
-        for zz in range(nz):
-            share_core(q, c, zz).wait_send()
-    for u in range(len(units)):
-        for zb in range(nz):
-            w_core(u, zb, c).wait_send()
-
-            @pl.when((z >= zb) & (z < nz - 1))
-            def _():
-                w_up(u, zb).wait_send()
-
-            @pl.when((z <= zb) & (z > 0))
-            def _():
-                w_dn(u, zb).wait_send()
-    for pt in peers_t:
-        rcopy(tsend, tbuf.at[t], t_s.at[pt], t_r.at[t], f, pt).wait_send()
+    for i in PAIR:
+        took(wg[i].at[pl.ds(0, nz)], wd_r.at[i])
+    weights_gone()
+    took(tbuf.at[pl.ds(0, nt - 1)], t_s.at[0])
 
 
 def gather_and_reduce(nf, nt, lefts, rights, weights, bases, means, squares):
@@ -539,27 +589,26 @@
     return pl.pallas_call(
         functools.partial(exchange, nf, nt),
         out_shape=(
-            *outs(lambda h, w: (nf, h, w)), *outs(lambda h, w: (nf, h, rank)), *outs(ranked),
+            *outs(lambda h, w: (nf, h, w)), *outs(lambda h, w: (nf * h, w), F32),
             *outs(ranked, F32), *outs(ranked, F32), *outs(lambda h, w: (h, w), F32),
             jax.ShapeDtypeStruct((2, 8, 128), F32),
         ),
         in_specs=[hbm] * 12,
-        out_specs=(vmem,) * 13,
+        out_specs=(vmem,) * 11,
         scratch_shapes=[
-            *[pltpu.VMEM(x.shape, x.dtype) for x in fetched],
+            *[pltpu.VMEM(x.shape, x.dtype) for x in fetched], *two(lambda h, w: (nf, h, rank)), *two(ranked),
             *four(halves), *four(halves), *four(halves, F32), *four(lambda w: (tokens, half)),
-            *four(lambda w: (nf, seg, w), F32), *four(pieces), *four(pieces), *four(pieces), *four(pieces),
+            *four(lambda w: (nf, seg, w), F32), *four(pieces), *four(pieces), *four(pieces),
+            *four(lambda w: (nz + 1, seg, w)),
             *four(lambda w: (nf, seg, w)),
             pltpu.VMEM((2, 8, 128), F32),
             pltpu.VMEM((nt, 2, 8, 128), F32),
-            dma((12,)), dma((3, nz)), dma((3, nz)), dma((3,)), dma((3,)),
-            dma((3, nz)), dma((3, nt)), dma((2, nz, nt)), dma((2, nz, nt)), dma((2, nf)), dma((2, nf)),
-            *[dma((units, nz))] * 5,
-            *[dma((4, 2, levels))] * 4,
-            dma((4,)), dma((4,)), *[dma((4, nz))] * 6, dma((nt,)), dma((nt,)),
+            dma((12,)), *[dma((3,))] * 6, *[dma((2, nz))] * 2, *[dma((2,))] * 2, dma((2,)), dma((2,)), dma((units, nz)), dma((2,)), dma((2,)),
+            dma((4,)), dma((4, levels)), dma((4,)), dma((4, levels)), dma((4,)), dma((4,)), dma((4,)), dma((4, 2)),
+            *[dma((4,))] * 4, dma((1,)), dma((1,)),
         ],
         compiler_params=pltpu.CompilerParams(
-            collective_id=0, has_side_effects=True, vmem_limit_bytes=40 * 1024 * 1024
+            collective_id=0, has_side_effects=True, vmem_limit_bytes=34 * 1024 * 1024
         ),
         name="exchange",
     )(*[pltpu.with_memory_space_constraint(x, pltpu.HBM)
@@ -567,11 +616,11 @@
 
 
 def apply(nf, nt, *refs):
-    wg, bg, dirs, mean_new, square_new, w32 = (refs[2 * k:2 * k + 2] for k in range(6))
-    totals = refs[12]
-    outs = [refs[13 + 5 * i:18 + 5 * i] for i in PAIR]
-    step, new, copy = (refs[23 + 2 * k:25 + 2 * k] for k in range(3))
-    sem, csem = refs[29:]
+    wg, full, mean_new, square_new, w32 = (refs[2 * k:2 * k + 2] for k in range(5))
+    totals = refs[10]
+    outs = [refs[11 + 5 * i:16 + 5 * i] for i in PAIR]
+    step, new, copy = (refs[21 + 2 * k:23 + 2 * k] for k in range(3))
+    sem, csem = refs[27:]
     f = lax.axis_index("fs")
 
     def to(k, i):
@@ -591,7 +640,8 @@
         count = w32[i].shape[0] * nf * w32[i].shape[1] * nt
         scale = LEARN_RATE * lax.rsqrt(totals[i, 0:1, 0:1] / lax.convert_element_type(count, F32) + EPS_RMS)
         scales.append(scale)
-        own = scale * jnp.dot(bg[i][f], dirs[i][...], preferred_element_type=F32)
+        height = w32[i].shape[0]
+        own = scale * full[i][pl.ds(pl.multiple_of(f * height, height), height), :]
         step[i][...] = own
         new[i][...] = w32[i][...] - own
         to(0, i).start()
@@ -599,8 +649,8 @@
     for i in PAIR:
         height = w32[i].shape[0]
         for g in range(nf):
-            update = jnp.dot(bg[i][g], dirs[i][...], preferred_element_type=F32)
-            copy[i][pl.ds(g * height, height), :] = (wg[i][g].astype(F32) - scales[i] * update).astype(BF16)
+            at = pl.ds(g * height, height)
+            copy[i][at, :] = (wg[i][g].astype(F32) - scales[i] * full[i][at, :]).astype(BF16)
             block(i, g).start()
     for i in PAIR:
         for k in (0, 1, 3, 4):
@@ -610,16 +660,16 @@
 
 
 def finish(nf, nt, gathered):
-    w32 = gathered[10:12]
+    w32 = gathered[8:10]
     vmem, hbm = pl.BlockSpec(memory_space=pltpu.VMEM), pl.BlockSpec(memory_space=pltpu.HBM)
     out_shape = []
     for i in PAIR:
         copy = jax.ShapeDtypeStruct((nf * w32[i].shape[0], w32[i].shape[1]), BF16)
         like = lambda x: jax.ShapeDtypeStruct(x.shape, F32)
-        out_shape += [like(w32[i]), like(w32[i]), copy, like(gathered[6 + i]), like(gathered[8 + i])]
+        out_shape += [like(w32[i]), like(w32[i]), copy, like(gathered[4 + i]), like(gathered[6 + i])]
     return pl.pallas_call(
         functools.partial(apply, nf, nt),
-        in_specs=[vmem] * 13,
+        in_specs=[vmem] * 11,
         out_specs=[hbm] * 10,
         out_shape=out_shape,
         scratch_shapes=[

time: 74.7 us -> 71.7 us (0.960)
  Pallas kernels: 73.9 us -> 70.9 us
    pallas_call x1, Pallas kernels: 69.2 us -> 66 us  [gather_and_reduce(): pl.pallas_call(functools.partial(exchange, nf, nt), out_shape=(*outs(lamb...]
where the time goes in v3:
time: 71.7 us; the launch traced here: 71.6 us
  Pallas kernels  70.9 us (99%)
    pallas_call x1, Pallas kernels, gather_and_reduce(): pl.pallas_call(functools.partial(exchange, nf, nt), out_shape=(*outs(lamb...  66 us
    pallas_call x1, Pallas kernels, finish(): pl.pallas_call(functools.partial(apply, nf, nt), in_specs=[vmem] * 11, ou...  4.9 us

profile of v3, /device:TPU:0, one launch (start us, length us, event | category | flops | bytes accessed | tf_op | source)
XLA Modules:
  0.0 71.6 jit_solution(4573845082818890233)
XLA Ops:
  0.6 66.0 %exchange.1 = (bf16[8,256,1024]{2,1,0:T(8,128)(2,1)S(1)}, bf16[8,128,512]{2,1,0:T(8,128)(2,1)S(1)}, f32[2048,1024]{1,0:T(8,128)S(1)}, f32[1024,512]{1,0:T(8,128)...) custom-call(bf16[1536,512]{1,0:T(8,128)(2,1)} %refs_0_.1, ...), custom_call_target="tpu_custom_call" | custom-call | tf_op jit(solution)/shard_map/exchange/pallas_call | solution.py:589
  66.7 4.9 %apply.1 = (f32[256,1024]{1,0:T(8,128)}, f32[256,1024]{1,0:T(8,128)}, bf16[2048,1024]{1,0:T(8,128)(2,1)}, f32[256,1024]{1,0:T(8,128)}, f32[256,1024]{1,0:T(8,128...) custom-call(bf16[8,256,1024]{2,1,0:T(8,128)(2,1)S(1)} %get-tuple-ele, ...), custom_call_target="tpu_custom_call" | custom-call | tf_op jit(solution)/shard_map/apply/pallas_call | solution.py:670

commit v4 on v3

--- a/solution.py
+++ b/solution.py
@@ -15,7 +15,7 @@
 F32, BF16 = jnp.float32, jnp.bfloat16
 PAIR = (0, 1)
 CORES = 2
-NEAR = (((1, 0), (1, 1)), ((1, 2), (1, 3)), ((1, 4), (2, 0)), ((2, 1),), ((2, 2),), ((2, 3),), ((2, 4),))
+NEAR = (((1, 0), (1, 1)), ((1, 2), (1, 3)), ((1, 4), (2, 0)), ((2, 1),), ((2, 2),), (), ((2, 3), (2, 4)))
 
 
 def rcopy(src, dst, send, recv, fs, tp):
@@ -537,11 +537,11 @@
         rest_take(i)
     direct(0)
     direct(1)
+    line_take(2)
+    line_take(3)
     for i in PAIR:
         rest_end(i)
     norm(0)
-    line_take(2)
-    line_take(3)
     direct(2)
     direct(3)
     norm(1)

time: 71.7 us -> 70.8 us (0.987)
  Pallas kernels: 70.9 us -> 70 us
    pallas_call x1, Pallas kernels: 66 us -> 65.1 us  [gather_and_reduce(): pl.pallas_call(functools.partial(exchange, nf, nt), out_shape=(*outs(lamb...]
where the time goes in v4:
time: 70.8 us; the launch traced here: 70.7 us
  Pallas kernels  70 us (99%)
    pallas_call x1, Pallas kernels, gather_and_reduce(): pl.pallas_call(functools.partial(exchange, nf, nt), out_shape=(*outs(lamb...  65.1 us
    pallas_call x1, Pallas kernels, finish(): pl.pallas_call(functools.partial(apply, nf, nt), in_specs=[vmem] * 11, ou...  4.9 us

profile of v4, /device:TPU:0, one launch (start us, length us, event | category | flops | bytes accessed | tf_op | source)
XLA Modules:
  0.0 70.7 jit_solution(5293151293026731672)
XLA Ops:
  0.6 65.1 %exchange.1 = (bf16[8,256,1024]{2,1,0:T(8,128)(2,1)S(1)}, bf16[8,128,512]{2,1,0:T(8,128)(2,1)S(1)}, f32[2048,1024]{1,0:T(8,128)S(1)}, f32[1024,512]{1,0:T(8,128)...) custom-call(bf16[1536,512]{1,0:T(8,128)(2,1)} %refs_0_.1, ...), custom_call_target="tpu_custom_call" | custom-call | tf_op jit(solution)/shard_map/exchange/pallas_call | solution.py:589
  65.8 4.9 %apply.1 = (f32[256,1024]{1,0:T(8,128)}, f32[256,1024]{1,0:T(8,128)}, bf16[2048,1024]{1,0:T(8,128)(2,1)}, f32[256,1024]{1,0:T(8,128)}, f32[256,1024]{1,0:T(8,128...) custom-call(bf16[8,256,1024]{2,1,0:T(8,128)(2,1)S(1)} %get-tuple-ele, ...), custom_call_target="tpu_custom_call" | custom-call | tf_op jit(solution)/shard_map/apply/pallas_call | solution.py:670

commit v5 on v4

--- a/solution.py
+++ b/solution.py
@@ -45,7 +45,7 @@
     left, right, mean, square, bg, dirs = (rest[2 * k:2 * k + 2] for k in range(6))
     sbuf, rbuf, kept, lifted, part, psend, pbuf, zsend, zbuf, tot = (rest[12 + 4 * k:16 + 4 * k] for k in range(10))
     (tsend, tbuf, isem, b_s, b_r, bd_s, bd_r, c_s, c_r, e_s, e_r, cd_s, cd_r, w_u, w_d, w_r, wd_s, wd_r,
-     rs_s, rs_r, ag_s, ag_r, p_s, p_r, z_s, z_r, g_s, g_r, gd_s, gd_r, t_s, t_r) = rest[52:]
+     rs_s, rs_r, ag_r, p_r, z_s, z_r, g_r, gd_r, t_s, t_r) = rest[52:]
 
     nz = nf // CORES
     f, t = lax.axis_index("fs"), lax.axis_index("tp")
@@ -213,7 +213,7 @@
 
     def ag(q, h, k):
         ref = lifted[q].at[rows(bases[h][k + 1], sizes[k + 1])]
-        return rcopy(ref, ref, ag_s.at[q], ag_r.at[q, k], f, mates[h][k])
+        return rcopy(ref, ref, rs_s.at[q], ag_r.at[q, k], f, mates[h][k])
 
     def senders(i, then):
         parts = parts_of(bg[i].shape[1], nt)
@@ -297,7 +297,7 @@
         for h in PAIR:
             contract(q, away(h, k))
 
-    pairs = [rcopy(psend[q], pbuf[q], p_s.at[q], p_r.at[q], partner, t) for q in range(4)]
+    pairs = [rcopy(psend[q], pbuf[q], z_s.at[q], p_r.at[q], partner, t) for q in range(4)]
     me = c * nz + z
 
     chained = (0, 1)
@@ -325,11 +325,11 @@
 
     def share(q, pz, at):
         ref = tot[q].at[at]
-        return rcopy(ref, ref, g_s.at[q], g_r.at[q], pz * CORES + c, t)
+        return rcopy(ref, ref, z_s.at[q], g_r.at[q], pz * CORES + c, t)
 
     def share_core(q):
         ref = tot[q].at[pl.ds(c * nz, nz)]
-        return rcopy(ref, ref, gd_s.at[q], gd_r.at[q], partner, t)
+        return rcopy(ref, ref, z_s.at[q], gd_r.at[q], partner, t)
 
     def pair_send(q):
         for zz in range(nz):
@@ -443,14 +443,10 @@
 
     def tokens_gone(q):
         sent = 2 * sum(sizes[1:])
-        took(lifted[q].at[pl.ds(0, sent)], rs_s.at[q])
-        took(lifted[q].at[pl.ds(0, sent)], ag_s.at[q])
+        took(kept[q].at[:, pl.ds(0, sent // 2)], rs_s.at[q])
 
     def line_gone(q):
-        pairs[q].wait_send()
-        took(zsend[q].at[pl.ds(0, nz - 1)], z_s.at[q])
-        took(tot[q].at[pl.ds(0, nz - 1)], g_s.at[q])
-        share_core(q).wait_send()
+        took(part[q].at[pl.ds(0, 2 * nz - 1)], z_s.at[q])
 
     def weights_gone():
         for i in PAIR:
@@ -604,8 +600,8 @@
             pltpu.VMEM((2, 8, 128), F32),
             pltpu.VMEM((nt, 2, 8, 128), F32),
             dma((12,)), *[dma((3,))] * 6, *[dma((2, nz))] * 2, *[dma((2,))] * 2, dma((2,)), dma((2,)), dma((units, nz)), dma((2,)), dma((2,)),
-            dma((4,)), dma((4, levels)), dma((4,)), dma((4, levels)), dma((4,)), dma((4,)), dma((4,)), dma((4, 2)),
-            *[dma((4,))] * 4, dma((1,)), dma((1,)),
+            dma((4,)), dma((4, levels)), dma((4, levels)), dma((4,)), dma((4,)), dma((4, 2)),
+            *[dma((4,))] * 2, dma((1,)), dma((1,)),
         ],
         compiler_params=pltpu.CompilerParams(
             collective_id=0, has_side_effects=True, vmem_limit_bytes=34 * 1024 * 1024

time: 70.8 us -> 70.7 us (level)
  no operation moved by 1% of the time
where the time goes in v5:
time: 70.7 us; the launch traced here: 70.6 us
  Pallas kernels  69.9 us (99%)
    pallas_call x1, Pallas kernels, gather_and_reduce(): pl.pallas_call(functools.partial(exchange, nf, nt), out_shape=(*outs(lamb...  65 us
    pallas_call x1, Pallas kernels, finish(): pl.pallas_call(functools.partial(apply, nf, nt), in_specs=[vmem] * 11, ou...  4.9 us

profile of v5, /device:TPU:0, one launch (start us, length us, event | category | flops | bytes accessed | tf_op | source)
XLA Modules:
  0.0 70.6 jit_solution(17243637514753366732)
XLA Ops:
  0.6 65.0 %exchange.1 = (bf16[8,256,1024]{2,1,0:T(8,128)(2,1)S(1)}, bf16[8,128,512]{2,1,0:T(8,128)(2,1)S(1)}, f32[2048,1024]{1,0:T(8,128)S(1)}, f32[1024,512]{1,0:T(8,128)...) custom-call(bf16[1536,512]{1,0:T(8,128)(2,1)} %refs_0_.1, ...), custom_call_target="tpu_custom_call" | custom-call | tf_op jit(solution)/shard_map/exchange/pallas_call | solution.py:585
  65.7 4.9 %apply.1 = (f32[256,1024]{1,0:T(8,128)}, f32[256,1024]{1,0:T(8,128)}, bf16[2048,1024]{1,0:T(8,128)(2,1)}, f32[256,1024]{1,0:T(8,128)}, f32[256,1024]{1,0:T(8,128...) custom-call(bf16[8,256,1024]{2,1,0:T(8,128)(2,1)S(1)} %get-tuple-ele, ...), custom_call_target="tpu_custom_call" | custom-call | tf_op jit(solution)/shard_map/apply/pallas_call | solution.py:666
